TPU v7x, 128 devices: a whole 4x4x4 slice. The times are simulated.
128 devices in a mesh: fs: 32 (over z, y, core), tp: 4 (over x).
Axes of the slice: x: 4, y: 4, z: 4, core: 2. Of those that a mesh axis runs over, the one named last changes fastest.
Arguments:
- first_map: bfloat16 [24576, 2048], P('fs', 'tp'), may hold values from -6 to 6
- second_map: bfloat16 [24576, 2048], P('fs', 'tp'), may hold values from -6 to 6
- lambda_head: float32 [16], P('tp'), may hold values from 0.3 to 0.8
- head_gain: float32 [2048], P('tp'), may hold values from 0.1 to 1.9
- cot_output: bfloat16 [24576, 4096], P('fs'), may hold values from -6 to 6
- layer_input: bfloat16 [24576, 4096], P('fs'), may hold values from -6 to 6
- cot_values: bfloat16 [24576, 2048], P('fs', 'tp'), may hold values from -16 to 16
- factor_value: bfloat16 [4096, 256], P('fs'), may hold values from -1 to 1
- factor_output: bfloat16 [4096, 256], P('fs'), may hold values from -1 to 1
- weight_value: float32 [4096, 2048], P('fs', 'tp'), may hold values from -6 to 6
- weight_output: float32 [2048, 4096], P('tp', 'fs'), may hold values from -6 to 6
- first_value: float32 [256, 2048], P('fs', 'tp'), may hold values from -6 to 6
- second_value: float32 [256, 2048], P('fs', 'tp'), may hold values from 0.05 to 1
- first_output: float32 [256, 2048], P('fs', 'tp'), may hold values from -6 to 6
- second_output: float32 [256, 2048], P('fs', 'tp'), may hold values from 0.05 to 1
Outputs:
- new_weight_value: float32 [4096, 2048], P('fs', 'tp')
- new_first_value: float32 [256, 2048], P('fs', 'tp')
- new_second_value: float32 [256, 2048], P('fs', 'tp')
- copy_value: bfloat16 [4096, 2048], P(None, 'tp')
- new_weight_output: float32 [2048, 4096], P('tp', 'fs')
- new_first_output: float32 [256, 2048], P('fs', 'tp')
- new_second_output: float32 [256, 2048], P('fs', 'tp')
- copy_output: bfloat16 [2048, 4096], P('tp')
All inputs are finite; a program needn't handle non-finite values.
Results may differ from a plain program's by a relative error of at most 0.002.
Values may be sent and summed in bfloat16 or wider, within the bound.
A program may use at most 128 MiB of HBM per device.

v0:
```python
import math

import jax
import jax.numpy as jnp
from jax import lax
from jax.sharding import Mesh
from jax.sharding import PartitionSpec as P

RANK = 256
HV = 2048
FS = ("fs_0", "fs_1", "fs_2")
FS_TP = ("fs_0", "fs_1", "fs_2", "tp")


norm_epsilon = 1e-06
first_decay = 0.9
second_decay = 0.95
learn_rate = 0.1


def in_blocks(value, dim, devices):
    dims = value.shape
    tiles = value.reshape(*dims[:dim], devices, dims[dim] // devices, *dims[dim + 1 :])
    return jnp.moveaxis(tiles, dim, 0)


def sent_and_summed(value, axis, dim):
    devices = lax.axis_size(axis)
    tiles = lax.all_to_all(in_blocks(value, dim, devices), axis, 0, 0, tiled=True)
    return jnp.sum(tiles, axis=0)


def side_by_side(arrays, axis, dim, along):
    ends, at = ([], 0)
    for a in arrays[:-1]:
        at += a.shape[along]
        ends.append(at)
    both = jnp.concatenate(arrays, axis=along)
    return tuple(jnp.split(lax.all_gather(both, axis, axis=dim, tiled=True), ends, axis=along))


def over_axes(value, axes):
    for axis in axes:
        value = lax.psum(value, axis)
    return value


def gather_turned(arrays, axis, dims):
    turned = [jnp.moveaxis(a, dim, 0) for a, dim in zip(arrays, dims)]
    both = jnp.concatenate([t.reshape(len(t), -1) for t in turned], axis=1)
    result, at, outs = (lax.all_gather(both, axis, axis=0, tiled=True), 0, [])
    for t, dim in zip(turned, dims):
        slab = result[:, at : at + t[0].size].reshape(-1, *t.shape[1:])
        outs.append(jnp.moveaxis(slab, 0, dim))
        at += t[0].size
    return tuple(outs)


def head_output(first_map, second_map, lambda_head, head_gain):
    heads_here = lambda_head.shape[0]
    head_width = first_map.shape[1] // heads_here
    count_rows = first_map.shape[0]
    spread = jnp.repeat(lambda_head, head_width)
    differ = first_map.astype(jnp.float32) - spread[None, :] * second_map.astype(jnp.float32)
    grouped = differ.reshape(count_rows, heads_here, head_width)
    scaled = grouped * lax.rsqrt(jnp.mean(grouped * grouped, -1, keepdims=True) + norm_epsilon)
    return (scaled.reshape(count_rows, heads_here * head_width) * head_gain[None, :]).astype(
        jnp.bfloat16
    )


def moments(projected, clip_factor, first_old, second_old):
    scaled = clip_factor * projected
    first_new = first_decay * first_old + (1.0 - first_decay) * scaled
    second_new = second_decay * second_old + (1.0 - second_decay) * scaled * scaled
    return (first_new, second_new, first_new * lax.rsqrt(second_new))


def low_rank(left, right):
    return sent_and_summed(
        lax.dot_general(
            left,
            right,
            (((0,), (0,)), ((), ())),
            precision=lax.Precision.HIGHEST,
            preferred_element_type=jnp.float32,
        ),
        FS,
        0,
    )


def shards(
    first_map,
    second_map,
    lambda_head,
    head_gain,
    cot_output,
    layer_input,
    cot_values,
    factor_value,
    factor_output,
    weight_value,
    weight_output,
    first_value,
    second_value,
    first_output,
    second_output,
):
    heads_out = head_output(first_map, second_map, lambda_head, head_gain)
    factor_v32 = factor_value.astype(jnp.float32)
    factor_o32 = factor_output.astype(jnp.float32)
    whole_value, whole_output = side_by_side((factor_value, factor_output), FS, 0, 1)
    mapped_value = jnp.dot(layer_input, whole_value, preferred_element_type=jnp.float32)
    mapped_output = jnp.dot(cot_output, whole_output, preferred_element_type=jnp.float32)
    low_value = low_rank(mapped_value, cot_values.astype(jnp.float32))
    low_output = low_rank(mapped_output, heads_out.astype(jnp.float32))
    partial_value = jnp.sum(low_value * low_value) + jnp.sum(low_output * low_output)
    total = over_axes(partial_value, FS_TP)
    clip_factor = jnp.minimum(1.0, math.sqrt(RANK * HV) * lax.rsqrt(total + norm_epsilon))
    first_v, second_v, ratio_value = moments(low_value, clip_factor, first_value, second_value)
    first_o, second_o, ratio_output = moments(low_output, clip_factor, first_output, second_output)
    pieces = side_by_side((ratio_value, ratio_output), FS, 0, 1)
    added_value = jnp.dot(
        factor_v32, pieces[0], precision=lax.Precision.HIGHEST, preferred_element_type=jnp.float32
    )
    added_output = lax.dot_general(
        pieces[1],
        factor_o32,
        (((0,), (1,)), ((), ())),
        precision=lax.Precision.HIGHEST,
        preferred_element_type=jnp.float32,
    )
    new_value = weight_value - learn_rate * added_value
    new_output = weight_output - learn_rate * added_output
    copy_value, copy_output = gather_turned(
        (new_value.astype(jnp.bfloat16), new_output.astype(jnp.bfloat16)), FS, (0, 1)
    )
    return (new_value, first_v, second_v, copy_value, new_output, first_o, second_o, copy_output)


def solution(mesh):
    torus = Mesh(mesh.devices.reshape(4, 4, 2, mesh.shape["tp"]), ("fs_0", "fs_1", "fs_2", "tp"))
    placed = (
        P(FS, "tp"),
        P(FS, "tp"),
        P("tp"),
        P("tp"),
        P(FS, None),
        P(FS, None),
        P(FS, "tp"),
        P(FS, None),
        P(FS, None),
        P(FS, "tp"),
        P("tp", FS),
        P(FS, "tp"),
        P(FS, "tp"),
        P(FS, "tp"),
        P(FS, "tp"),
    )
    return jax.shard_map(
        shards,
        mesh=torus,
        in_specs=placed,
        out_specs=(
            P(FS, "tp"),
            P(FS, "tp"),
            P(FS, "tp"),
            P(None, "tp"),
            P("tp", FS),
            P(FS, "tp"),
            P(FS, "tp"),
            P("tp", None),
        ),
        check_vma=False,
    )
```

profile of v0, /device:TPU:1, one launch (start us, length us, event | category | flops | bytes accessed | tf_op | source)
XLA Modules:
  0.0 256.5 jit_solution(15353092697436282198)
XLA Ops:
  7.2 0.0 copy-start
  7.2 0.0 all-gather.4.cloned.1.call-start
  7.2 1.6 pad_maximum_fusion.1
  8.8 0.0 all-gather.4.cloned.1.call-update
  8.9 0.7 broadcast_bitcast_fusion
  9.6 2.8 %fusion.6 = f32[768,512]{1,0:T(8,128)} fusion(bf16[768,512]{1,0:T(8,128)(2,1)} %param.16, bf16[768,512]{1,0:T(8,128)(2,1)} %param.15, f32[512]{0:T(512)S(1)} %broadcast_bitcast_fusion), kind=kLoop, calls=%fused_computation.9 | loop fusion | flops 1966080 | bytes 3147776 | tf_op jit(solution)/shard_map/mul | solution.py:66
  12.4 1.8 mul.106
  14.1 0.9 reduce_sum.47
  15.0 0.1 add_rsqrt_fusion
  15.1 45.5 %all-gather.4.cloned.1.call-done = bf16[4096,512]{1,0:T(8,128)(2,1)} async-done(((bf16[128,512]{1,0:T(8,128)(2,1)}), bf16[4096,512]{1,0:T(8,128)(2,1)}) %all-gather.4.cloned.1.call-update) | async-done | bytes 4194320 | tf_op jit(solution)/shard_map/all_gather | solution.py:39
  60.6 5.3 %fusion.2 = f32[256,768]{1,0:T(8,128)S(1)} fusion(bf16[768,4096]{1,0:T(8,128)(2,1)} %param.20, bf16[4096,512]{1,0:T(8,128)(2,1)} %all-gather.4.cloned.1.call-done), kind=kOutput, calls=%fused_computation.3 | convolution fusion | flops 1610612736 | bytes 9175040 | tf_op jit(solution)/shard_map/dot_general | solution.py:114
  65.9 1.6 convolution_bitcast_fusion
  67.5 5.3 %all-to-all-start = ((f32[32,8,512]{2,1,0:T(8,128)}), f32[32,8,512]{2,1,0:T(8,128)S(1)}, u32[]{:S(2)}, u32[]{:S(2)}) async-start(f32[32,8,512]{2,1,0:T(8,128)} %convolution_bitcast_fusion), calls=%async_computation | async-start | bytes 1048576 | tf_op jit(solution)/shard_map/all_to_all | solution.py:29
  72.8 0.0 copy-start.12
  72.8 5.3 %fusion.7 = f32[32,8,768]{2,1,0:T(8,128)S(1)} fusion(bf16[768,4096]{1,0:T(8,128)(2,1)} %param.19, bf16[4096,512]{1,0:T(8,128)(2,1)} %all-gather.4.cloned.1.call-done), kind=kOutput, calls=%fused_computation.10 | convolution fusion | flops 1610612736 | bytes 9175040 | tf_op jit(solution)/shard_map/dot_general | solution.py:115
  78.1 0.0 copy-start.1
  78.1 0.0 copy-start.2
  78.1 1.0 mul.107
  79.1 0.1 copy-done.1
  79.2 0.2 copy-done.2
  79.5 1.8 fusion.14
  81.3 0.0 copy-start.5
  81.3 0.0 copy-start.4
  81.3 0.0 copy-start.6
  81.4 2.9 %all-to-all-done = f32[32,8,512]{2,1,0:T(8,128)S(1)} async-done(((f32[32,8,512]{2,1,0:T(8,128)}), f32[32,8,512]{2,1,0:T(8,128)S(1)}, u32[]{:S(2)}, u32[]{:S(2)}) %all-to-all-start) | async-done | bytes 524320 | tf_op jit(solution)/shard_map/all_to_all | solution.py:29
  84.2 4.6 %all-to-all-start.1 = ((f32[32,8,512]{2,1,0:T(8,128)}), f32[32,8,512]{2,1,0:T(8,128)S(1)}, u32[]{:S(2)}, u32[]{:S(2)}) async-start(f32[32,8,512]{2,1,0:T(8,128)} %fusion.14), calls=%async_computation.1 | async-start | bytes 1048576 | tf_op jit(solution)/shard_map/all_to_all | solution.py:29
  88.9 0.0 all-gather.6.cloned.1.call-start
  89.0 0.6 multiply_reduce_fusion.1
  89.6 10.7 %all-to-all-done.1 = f32[32,8,512]{2,1,0:T(8,128)S(1)} async-done(((f32[32,8,512]{2,1,0:T(8,128)}), f32[32,8,512]{2,1,0:T(8,128)S(1)}, u32[]{:S(2)}, u32[]{:S(2)}) %all-to-all-start.1) | async-done | bytes 524320 | tf_op jit(solution)/shard_map/all_to_all | solution.py:29
  100.4 0.6 multiply_reduce_fusion
  102.3 7.4 %psum.28 = f32[]{:T(128)} all-reduce(f32[]{:T(128)S(6)} %add.39), channel_id=1, replica_groups=mesh['fs_0'=4,'fs_1'=4,'fs_2'=2,'tp'=4] {'fs_0'}, use_global_device_ids=true, to_apply=%region_5.0 | all-reduce | flops 1 | bytes 8 | tf_op jit(solution)/shard_map/psum | solution.py:44
  109.6 8.4 %psum.29 = f32[]{:T(128)} all-reduce(f32[]{:T(128)} %psum.28), channel_id=1, replica_groups=mesh['fs_0'=4,'fs_1'=4,'fs_2'=2,'tp'=4] {'fs_1'}, use_global_device_ids=true, to_apply=%region_6.0 | all-reduce | flops 1 | bytes 8 | tf_op jit(solution)/shard_map/psum | solution.py:44
  118.1 5.8 %psum.30 = f32[]{:T(128)} all-reduce(f32[]{:T(128)} %psum.29), channel_id=1, replica_groups=mesh['fs_0'=4,'fs_1'=4,'fs_2'=2,'tp'=4] {'fs_2'}, use_global_device_ids=true, to_apply=%region_7.0 | all-reduce | flops 1 | bytes 8 | tf_op jit(solution)/shard_map/psum | solution.py:44
  123.9 9.0 %psum.31 = f32[]{:T(128)} all-reduce(f32[]{:T(128)} %psum.30), channel_id=1, replica_groups=mesh['fs_0'=4,'fs_1'=4,'fs_2'=2,'tp'=4] {'tp'}, use_global_device_ids=true, to_apply=%region_8.0 | all-reduce | flops 1 | bytes 8 | tf_op jit(solution)/shard_map/psum | solution.py:44
  133.6 0.6 rsqrt_multiply_fusion
  134.3 0.6 pad_maximum_fusion.2
  134.9 0.0 all-gather.6.cloned.1.call-update
  134.9 0.0 all-gather.8.cloned.1.call-start
  135.0 0.1 copy.32
  135.1 39.8 %all-gather.6.cloned.1.call-done = f32[256,1024]{1,0:T(8,128)} async-done(((f32[8,1024]{1,0:T(8,128)}), f32[256,1024]{1,0:T(8,128)}) %all-gather.6.cloned.1.call-update) | async-done | bytes 1048592 | tf_op jit(solution)/shard_map/all_gather | solution.py:39
  175.0 1.7 fusion.10
  176.7 1.7 fusion.24
  178.4 0.7 pad_maximum_fusion
  179.1 0.0 all-gather.8.cloned.1.call-update
  179.1 0.8 copy.33
  180.0 57.5 %all-gather.8.cloned.1.call-done = bf16[4096,1024]{0,1:T(8,128)(2,1)} async-done(((bf16[128,1024]{0,1:T(8,128)(2,1)}), bf16[4096,1024]{0,1:T(8,128)(2,1)}) %all-gather.8.cloned.1.call-update) | async-done | bytes 8388624 | tf_op jit(solution)/shard_map/all_gather | solution.py:51
  237.5 6.0 %slice_bitcast_fusion = (bf16[512,4096]{1,0:T(8,128)(2,1)}, bf16[4096,512]{0,1:T(8,128)(2,1)}) fusion(bf16[4096,1024]{0,1:T(8,128)(2,1)} %all-gather.8.cloned.1.call-done), kind=kLoop, calls=%fused_computation | loop fusion | bytes 16777216 | tf_op jit(solution)/shard_map/transpose | solution.py:54
  243.5 6.4 %copy.34 = bf16[4096,512]{1,0:T(8,128)(2,1)} copy(bf16[4096,512]{0,1:T(8,128)(2,1)} %get-tuple-element.39) | data formatting | bytes 8388608
  (20 shorter events, 0.1 us)
Async XLA Ops:
  7.2 58.7 %copy-start = (bf16[768,512]{1,0:T(8,128)(2,1)S(1)}, bf16[768,512]{1,0:T(8,128)(2,1)}, u32[]{:S(2)}) copy-start(bf16[768,512]{1,0:T(8,128)(2,1)} %param.21) | copy-start | bytes 2359300
  7.2 53.5 %all-gather.4.cloned.1.call-start = ((), (), s32[]{:S(2)}) async-start(), calls=%async_computation.2 | async-start | bytes 4325376 | tf_op jit(solution)/shard_map/all_gather | solution.py:39
  67.5 16.7 %all-to-all-start = ((f32[32,8,512]{2,1,0:T(8,128)}), f32[32,8,512]{2,1,0:T(8,128)S(1)}, u32[]{:S(2)}, u32[]{:S(2)}) async-start(f32[32,8,512]{2,1,0:T(8,128)} %convolution_bitcast_fusion), calls=%async_computation | async-start | bytes 1048576 | tf_op jit(solution)/shard_map/all_to_all | solution.py:29
  72.8 6.3 %copy-start.12 = (f32[512]{0:T(512)S(1)}, f32[512]{0:T(512)}, u32[]{:S(2)}) copy-start(f32[512]{0:T(512)} %param.18) | copy-start | bytes 6148
  78.1 1.1 copy-start.1
  78.1 1.4 copy-start.2
  81.3 52.3 %copy-start.8 = (f32[8,512]{1,0:T(8,128)S(1)}, f32[8,512]{1,0:T(8,128)}, u32[]{:S(2)}) copy-start(f32[8,512]{1,0:T(8,128)} %param.29) | copy-start | bytes 49156
  81.3 52.3 %copy-start.9 = (f32[8,512]{1,0:T(8,128)S(1)}, f32[8,512]{1,0:T(8,128)}, u32[]{:S(2)}) copy-start(f32[8,512]{1,0:T(8,128)} %param.28) | copy-start | bytes 49156
  81.3 52.3 %copy-start.10 = (f32[8,512]{1,0:T(8,128)S(1)}, f32[8,512]{1,0:T(8,128)}, u32[]{:S(2)}) copy-start(f32[8,512]{1,0:T(8,128)} %param.27) | copy-start | bytes 49156
  81.3 52.3 %copy-start.11 = (f32[8,512]{1,0:T(8,128)S(1)}, f32[8,512]{1,0:T(8,128)}, u32[]{:S(2)}) copy-start(f32[8,512]{1,0:T(8,128)} %param.26) | copy-start | bytes 49156
  81.3 53.7 %copy-start.5 = (f32[128,512]{1,0:T(8,128)S(1)}, f32[128,512]{1,0:T(8,128)}, u32[]{:S(2)}) copy-start(f32[128,512]{1,0:T(8,128)} %param.24) | copy-start | bytes 786436
  81.3 93.6 %copy-start.4 = (f32[512,128]{1,0:T(8,128)S(1)}, f32[512,128]{1,0:T(8,128)}, u32[]{:S(2)}) copy-start(f32[512,128]{1,0:T(8,128)} %param.25) | copy-start | bytes 786436
  81.3 93.6 %copy-start.6 = (bf16[128,256]{1,0:T(8,128)(2,1)S(1)}, bf16[128,256]{1,0:T(8,128)(2,1)}, u32[]{:S(2)}) copy-start(bf16[128,256]{1,0:T(8,128)(2,1)} %param.23) | copy-start | bytes 196612
  81.3 95.3 %copy-start.7 = (bf16[128,256]{1,0:T(8,128)(2,1)S(1)}, bf16[128,256]{1,0:T(8,128)(2,1)}, u32[]{:S(2)}) copy-start(bf16[128,256]{1,0:T(8,128)(2,1)} %param.22) | copy-start | bytes 196612
  84.2 16.1 %all-to-all-start.1 = ((f32[32,8,512]{2,1,0:T(8,128)}), f32[32,8,512]{2,1,0:T(8,128)S(1)}, u32[]{:S(2)}, u32[]{:S(2)}) async-start(f32[32,8,512]{2,1,0:T(8,128)} %fusion.14), calls=%async_computation.1 | async-start | bytes 1048576 | tf_op jit(solution)/shard_map/all_to_all | solution.py:29
  88.9 86.1 %all-gather.6.cloned.1.call-start = ((), (), s32[]{:S(2)}) async-start(), calls=%async_computation.3 | async-start | bytes 1081344 | tf_op jit(solution)/shard_map/all_gather | solution.py:39
  134.9 102.6 %all-gather.8.cloned.1.call-start = ((), (), s32[]{:S(2)}) async-start(), calls=%async_computation.4 | async-start | bytes 8650752 | tf_op jit(solution)/shard_map/all_gather | solution.py:51
  176.6 66.9 %copy-start.3 = (f32[512,128]{1,0:T(8,128)}, f32[512,128]{1,0:T(8,128)S(1)}, u32[]{:S(2)}) copy-start(f32[512,128]{1,0:T(8,128)S(1)} %fusion.10) | copy-start | bytes 786436
Sparse Core Ops, SparseCore 0:
  10.8 49.7 all-gather.3
  135.0 39.8 all-gather.5
  179.2 58.2 all-gather.7
where the time goes:
time: 257 us; the launch traced here: 256 us
  waiting for transfers between devices  157 us (61%)
  blocking collectives  30.6 us (12%)
  local copies, waits for them, and re-layouts  17.3 us (7%)
  matrix products  17.3 us (7%)
  between operations  16 us (6%)
  starting transfers between devices  10.1 us (4%)
  other arithmetic  8.61 us (3%)
    all_gather x2, waiting for transfers between devices, side_by_side(): lax.all_gather(both, axis, axis=dim, tiled=True)  85.4 us
    all_gather x1, waiting for transfers between devices, gather_turned(): result, at, outs = (lax.all_gather(both, axis, axis=0, tiled=True), 0, [])  57.5 us
    psum x4, blocking collectives, over_axes(): value = lax.psum(value, axis)  30.6 us
    all_to_all x2, waiting for transfers between devices, sent_and_summed(): lax.all_to_all(in_blocks(value, dim, devices), axis, 0, 0, tiled=True)  13.6 us
    all_to_all x2, starting transfers between devices, sent_and_summed(): lax.all_to_all(in_blocks(value, dim, devices), axis, 0, 0, tiled=True)  9.94 us
    unnamed x29, local copies, waits for them, and re-layouts  7.8 us
    transpose x1, local copies, waits for them, and re-layouts, gather_turned(): outs.append(jnp.moveaxis(slab, 0, dim))  6.03 us
    dot_general x1, matrix products, shards(): jnp.dot(cot_output, whole_output, preferred_element_type=jnp.float32)  5.27 us
  transfers between devices with their start and end apart: 5, of which 5 were waited for; matrix products, arithmetic and copies ran while one was open for 6% of the time, Pallas kernels for 0%

commit v1 on v0

v1 whole, which is shorter than its diff:
```python
import math

import jax
import jax.numpy as jnp
from jax import lax
from jax.experimental import pallas as pl
from jax.experimental.pallas import tpu as pltpu
from jax.sharding import Mesh
from jax.sharding import PartitionSpec as P

MESH = pl.DeviceIdType.MESH
RANK = 256
HV = 2048
FS = ("z", "y", "c")

norm_epsilon = 1e-06
first_decay = 0.9
second_decay = 0.95
learn_rate = 0.1

ROWS = 768
WIDE = 4096
COLS = 512
HEADS_HERE = 4
CHIPS = 16

f32 = jnp.float32
bf16 = jnp.bfloat16


def split_dot(left, right, dims):
    high = right.astype(bf16)
    low = (right - high.astype(f32)).astype(bf16)
    return lax.dot_general(left, high, dims, preferred_element_type=f32) + lax.dot_general(
        left, low, dims, preferred_element_type=f32
    )


def step_kernel(
    first_map, second_map, lambda_head, head_gain, cot_output, layer_input, cot_values,
    factor_value, factor_output, weight_value, weight_output,
    first_value, second_value, first_output, second_output,
    new_value, new_output, moved, copy_value, copy_output,
    maps, lam, gain, wide, cots, heads, factors, weights_v, weights_o, old,
    acc, lows, pair_in, summed, cross_in, squares, cross_sq, last_sq, ratios,
    load_sem, send_sem, recv_sem, pass_sem, pair_sem, cross_sem, sq_sem, last_sem,
):
    z, y, c, x = (lax.axis_index(a) for a in ("z", "y", "c", "x"))
    own = 4 * z + y
    partner = (z, y, 1 - c, x)

    def near(z_by, y_by, c_by, x_by):
        return (
            lax.rem(z + z_by, 4), lax.rem(y + y_by, 4), lax.rem(c + c_by, 2), lax.rem(x + x_by, 4)
        )

    def place(da, db, core):
        da, db = da % 4, db % 4
        return 4 * lax.rem(z + da * core + db * (1 - core), 4) + lax.rem(
            y + da * (1 - core) + db * core, 4
        )

    def chip_at(da, db):
        return near(da * c + db * (1 - c), da * (1 - c) + db * c, 0, 0)

    def load(k, source, target):
        copy = pltpu.make_async_copy(source, target, load_sem.at[k])
        copy.start()
        return copy

    own_factors = [
        load(0, factor_value, factors.at[0, own, c]),
        load(1, factor_output, factors.at[1, own, c]),
    ]
    barrier = pltpu.get_barrier_semaphore()
    greeted = [chip_at(1, 0), chip_at(3, 0), chip_at(0, 1), chip_at(0, 3), partner]
    greeted += [near(0, 0, dc, dx) for dx in (1, 2, 3) for dc in (0, 1)]
    for device in greeted:
        pl.semaphore_signal(barrier, inc=1, device_id=device, device_id_type=MESH)
    load_maps = [
        load(2, first_map, maps.at[0]),
        load(3, second_map, maps.at[1]),
        load(4, lambda_head, lam),
        load(5, head_gain, gain),
    ]
    load_wide = [load(6, layer_input, wide.at[0]), load(7, cot_output, wide.at[1])]
    load_rest = [
        load(8, cot_values, cots),
        load(9, weight_value, weights_v),
        load(10, weight_output, weights_o),
        load(11, first_value, old.at[0]),
        load(12, second_value, old.at[1]),
        load(13, first_output, old.at[2]),
        load(14, second_output, old.at[3]),
    ]
    for copy in own_factors:
        copy.wait()
    pl.semaphore_wait(barrier, len(greeted))

    class Gather:
        def __init__(self, stage, half):
            self.stage, self.half, self.sent = stage, half, []

        def fire(self, h, da, db, way):
            block = self.half(h, place(da, db, c), c)
            k = len(self.sent)
            ra, rb = da % 4, db % 4
            if way == "d":
                device, arrived = partner, pass_sem.at[self.stage, h, 4 * ra + rb]
            else:
                by = 1 if way[1] == "+" else 3
                if way[0] == "a":
                    device, ra = chip_at(by, 0), (ra - by) % 4
                else:
                    device, rb = chip_at(0, by), (rb - by) % 4
                arrived = recv_sem.at[self.stage, h, 4 * ra + rb]
            copy = pltpu.make_async_remote_copy(
                block, block, send_sem.at[k], arrived, device_id=device, device_id_type=MESH
            )
            copy.start()
            self.sent.append(copy)

        def start(self, h):
            for way in ("a+", "a-", "b+", "b-", "d"):
                self.fire(h, 0, 0, way)

        def wait(self, h, da, db):
            block = self.half(h, place(da, db, c), c)
            pltpu.make_async_remote_copy(
                block, block, send_sem.at[0], recv_sem.at[self.stage, h, 4 * (da % 4) + db % 4],
                device_id=partner, device_id_type=MESH,
            ).wait_recv()

        def take(self, h, da, db):
            self.wait(h, da, db)
            if db % 4 == 0:
                if da % 4 == 3 and h == 0:
                    self.fire(h, da, db, "a+")
                if da % 4 == 1 and h == 1:
                    self.fire(h, da, db, "a-")
                self.fire(h, da, db, "b+")
                self.fire(h, da, db, "b-")
            if db % 4 == 3 and h == 0:
                self.fire(h, da, db, "b+")
            if db % 4 == 1 and h == 1:
                self.fire(h, da, db, "b-")
            self.fire(h, da, db, "d")

        def take_all(self, places):
            for da, db in places:
                for h in (0, 1):
                    self.take(h, da, db)

        def wait_across(self, places):
            for da, db in places:
                for h in (0, 1):
                    block = self.half(h, place(da, db, 1 - c), 1 - c)
                    pltpu.make_async_remote_copy(
                        block, block, send_sem.at[0],
                        pass_sem.at[self.stage, h, 4 * (da % 4) + db % 4],
                        device_id=partner, device_id_type=MESH,
                    ).wait_recv()

        def wait_sent(self):
            for copy in self.sent:
                copy.wait_send()

    LEVELS = (
        ((0, 0),),
        ((3, 0), (1, 0), (0, 3), (0, 1)),
        ((2, 0), (3, 3), (3, 1), (1, 3), (1, 1), (0, 2)),
        ((2, 3), (2, 1), (3, 2), (1, 2)),
        ((2, 2),),
    )

    gather = Gather(0, lambda h, p, core: factors.at[h, p, core])
    gather.start(0)
    gather.start(1)

    for copy in load_maps:
        copy.wait()
    width = COLS // HEADS_HERE
    for h in range(HEADS_HERE):
        span = pl.ds(h * width, width)
        differ = maps[0, :, span].astype(f32) - lam[h] * maps[1, :, span].astype(f32)
        mean = jnp.sum(differ * differ, axis=-1, keepdims=True) * (1.0 / width)
        scaled = differ * lax.rsqrt(mean + norm_epsilon)
        heads[:, span] = (scaled * gain[span][None, :]).astype(bf16)

    def project(p, fresh):
        columns = pl.ds(pl.multiple_of(p * 256, 256), 256)
        for m in (0, 1):
            part = jnp.dot(
                wide[m, :, columns], factors[m, p].reshape(256, RANK), preferred_element_type=f32
            )
            acc[m] = part if fresh else acc[m] + part

    def at(dz, dy):
        return 4 * lax.rem(z + dz, 4) + lax.rem(y + dy, 4)

    def project_some(count, where):
        def body(i, carry):
            project(at(*where(i)), False)
            return carry

        lax.fori_loop(0, count, body, 0)

    gather.take_all(LEVELS[1])
    for copy in load_wide:
        copy.wait()
    gather.wait_across(LEVELS[0])
    project(own, True)
    gather.take_all(LEVELS[2])
    gather.wait_across(LEVELS[1])
    project_some(4, lambda i: ((1 - i // 2) * (1 + 2 * (i % 2)), (i // 2) * (1 + 2 * (i % 2))))
    gather.take_all(LEVELS[3])
    gather.wait_across(LEVELS[2])
    project_some(2, lambda i: (2 * (1 - i), 2 * i))
    project_some(4, lambda i: (1 + 2 * (i // 2), 1 + 2 * (i % 2)))
    gather.wait_across(LEVELS[3])
    project_some(
        4,
        lambda i: (
            (1 - i // 2) * 2 + (i // 2) * (1 + 2 * (i % 2)),
            (1 - i // 2) * (1 + 2 * (i % 2)) + (i // 2) * 2,
        ),
    )
    gather.take_all(LEVELS[4])
    gather.wait_across(LEVELS[4])
    project(at(2, 2), False)

    for copy in load_rest:
        copy.wait()
    pair = []
    for m in (0, 1):
        turned = acc[m].T
        high = turned.astype(bf16)
        low = (turned - high.astype(f32)).astype(bf16)
        right = (cots if m == 0 else heads)[...]
        product = jnp.dot(high, right, preferred_element_type=f32) + jnp.dot(
            low, right, preferred_element_type=f32
        )
        product = product.reshape(CHIPS, 2, 8, COLS)
        for core in (0, 1):
            lows[core, m] = product[:, core]
        copy = pltpu.make_async_remote_copy(
            lows.at[1 - c, m], pair_in.at[m], pair_sem.at[0, m], pair_sem.at[1, m],
            device_id=partner, device_id_type=MESH,
        )
        copy.start()
        pair.append(copy)
    gather.wait_sent()
    for m in (0, 1):
        pair[m].wait_recv()
        summed[:, m] = lows[c, m] + pair_in[m]
    for copy in pair:
        copy.wait_send()

    offsets = sorted(
        ((dz, dy) for dz in range(4) for dy in range(4) if (dz, dy) != (0, 0)),
        key=lambda o: -(min(o[0], 4 - o[0]) + min(o[1], 4 - o[1])),
    )
    cross = []
    for k, (dz, dy) in enumerate(offsets):
        copy = pltpu.make_async_remote_copy(
            summed.at[at(dz, dy)], cross_in.at[k], cross_sem.at[0, k], cross_sem.at[1, k],
            device_id=near(dz, dy, 0, 0), device_id_type=MESH,
        )
        copy.start()
        cross.append(copy)
    total = summed[own]
    for k in reversed(range(len(cross))):
        cross[k].wait_recv()
        total = total + cross_in[k]

    def fold(value):
        value = value.reshape(-1, 8, COLS)
        value = jnp.sum(value, axis=0)
        return sum(value[:, 128 * j : 128 * (j + 1)] for j in range(COLS // 128))

    squares[0] = fold(total * total)
    sent = []
    for k, (dz, dy) in enumerate(offsets):
        copy = pltpu.make_async_remote_copy(
            squares.at[0], cross_sq.at[k], sq_sem.at[0, k], sq_sem.at[1, k],
            device_id=near(dz, dy, 0, 0), device_id_type=MESH,
        )
        copy.start()
        sent.append(copy)
    for copy in cross:
        copy.wait_send()
    plane = squares[0]
    for k in reversed(range(len(sent))):
        sent[k].wait_recv()
        plane = plane + cross_sq[k]
    squares[1] = plane
    last = []
    for k, (dx, dc) in enumerate(((2, 1), (1, 1), (3, 1), (2, 0), (1, 0), (3, 0), (0, 1))):
        copy = pltpu.make_async_remote_copy(
            squares.at[1], last_sq.at[k], last_sem.at[0, k], last_sem.at[1, k],
            device_id=near(0, 0, dc, dx), device_id_type=MESH,
        )
        copy.start()
        last.append(copy)
    for copy in sent:
        copy.wait_send()
    whole = squares[1]
    for k in reversed(range(len(last))):
        last[k].wait_recv()
        whole = whole + last_sq[k]
    for copy in last:
        copy.wait_send()
    square_sum = jnp.sum(jnp.sum(whole, axis=1, keepdims=True), axis=0, keepdims=True)
    clip = jnp.minimum(1.0, math.sqrt(RANK * HV) * lax.rsqrt(square_sum + norm_epsilon))

    for m in (0, 1):
        scaled = clip * total[m]
        first_new = first_decay * old[2 * m] + (1.0 - first_decay) * scaled
        second_new = second_decay * old[2 * m + 1] + (1.0 - second_decay) * scaled * scaled
        moved[2 * m] = first_new
        moved[2 * m + 1] = second_new
        ratios[m, own, c] = first_new * lax.rsqrt(second_new)
    gather = Gather(1, lambda h, p, core: ratios.at[h, p, core])
    gather.start(0)
    gather.start(1)
    for level in LEVELS[1:]:
        gather.take_all(level)
    for level in LEVELS:
        gather.wait_across(level)
    gather.wait_sent()

    spread = Gather(
        2,
        lambda h, p, core: copy_value.at[p, core] if h == 0 else copy_output.at[p, core],
    )
    plain = (((1,), (0,)), ((), ()))
    added = split_dot(factors[0, own, c], ratios[0].reshape(RANK, COLS), plain)
    fresh = weights_v[...] - learn_rate * added
    copy_value[own, c] = fresh.astype(bf16)
    spread.start(0)
    new_value[...] = fresh
    added = split_dot(factors[1, own, c], ratios[1].reshape(RANK, COLS), plain)
    fresh = weights_o[...] - learn_rate * added.T
    copy_output[own, c] = fresh.astype(bf16)
    spread.start(1)
    new_output[...] = fresh
    for level in LEVELS[1:]:
        spread.take_all(level)
    for level in LEVELS:
        spread.wait_across(level)
    spread.wait_sent()


def write_kernel(new_value, new_output, moved, copy_value, copy_output, *rest):
    outs, sem = rest[:8], rest[8]
    new_v, first_v, second_v, copy_v, new_o, first_o, second_o, copy_o = outs
    pairs = [(copy_value, copy_v)]
    pairs += [
        (copy_output.at[k], copy_o.at[:, pl.ds(128 * k, 128)]) for k in range(copy_output.shape[0])
    ]
    pairs += [(new_value, new_v), (new_output, new_o)]
    pairs += [(moved.at[k], out) for k, out in enumerate((first_v, second_v, first_o, second_o))]
    copies = [pltpu.make_async_copy(s, t, sem.at[k]) for k, (s, t) in enumerate(pairs)]
    for copy in copies:
        copy.start()
    for copy in copies:
        copy.wait()


def shards(*args):
    any_space = pl.BlockSpec(memory_space=pltpu.HBM)
    vmem = pl.BlockSpec(memory_space=pltpu.VMEM)
    dma = pltpu.SemaphoreType.DMA
    new_value, new_output, moved, copy_value, copy_output = pl.pallas_call(
        step_kernel,
        out_shape=(
            pltpu.VMEM((128, COLS), f32),
            pltpu.VMEM((COLS, 128), f32),
            pltpu.VMEM((4, 8, COLS), f32),
            pltpu.VMEM((CHIPS, 2, 128, COLS), bf16),
            pltpu.VMEM((CHIPS, 2, COLS, 128), bf16),
        ),
        in_specs=[any_space] * 15,
        out_specs=(vmem,) * 5,
        scratch_shapes=[
            pltpu.VMEM((2, ROWS, COLS), bf16),
            pltpu.SMEM((HEADS_HERE,), f32),
            pltpu.VMEM((COLS,), f32),
            pltpu.VMEM((2, ROWS, WIDE), bf16),
            pltpu.VMEM((ROWS, COLS), bf16),
            pltpu.VMEM((ROWS, COLS), bf16),
            pltpu.VMEM((2, CHIPS, 2, 128, RANK), bf16),
            pltpu.VMEM((128, COLS), f32),
            pltpu.VMEM((COLS, 128), f32),
            pltpu.VMEM((4, 8, COLS), f32),
            pltpu.VMEM((2, ROWS, RANK), f32),
            pltpu.VMEM((2, 2, CHIPS, 8, COLS), f32),
            pltpu.VMEM((2, CHIPS, 8, COLS), f32),
            pltpu.VMEM((CHIPS, 2, 8, COLS), f32),
            pltpu.VMEM((15, 2, 8, COLS), f32),
            pltpu.VMEM((2, 8, 128), f32),
            pltpu.VMEM((15, 8, 128), f32),
            pltpu.VMEM((7, 8, 128), f32),
            pltpu.VMEM((2, CHIPS, 2, 8, COLS), f32),
            dma((15,)),
            dma((64,)),
            dma((3, 2, 16)),
            dma((3, 2, 16)),
            dma((2, 2)),
            dma((2, 15)),
            dma((2, 15)),
            dma((2, 7)),
        ],
        compiler_params=pltpu.CompilerParams(
            collective_id=0, has_side_effects=True, vmem_limit_bytes=46 * 1024 * 1024
        ),
        name="step",
    )(*args)
    return pl.pallas_call(
        write_kernel,
        out_shape=(
            jax.ShapeDtypeStruct((128, COLS), f32),
            jax.ShapeDtypeStruct((8, COLS), f32),
            jax.ShapeDtypeStruct((8, COLS), f32),
            jax.ShapeDtypeStruct((WIDE, COLS), bf16),
            jax.ShapeDtypeStruct((COLS, 128), f32),
            jax.ShapeDtypeStruct((8, COLS), f32),
            jax.ShapeDtypeStruct((8, COLS), f32),
            jax.ShapeDtypeStruct((COLS, WIDE), bf16),
        ),
        in_specs=[vmem] * 5,
        out_specs=(any_space,) * 8,
        scratch_shapes=[dma((2 * CHIPS + 7,))],
        compiler_params=pltpu.CompilerParams(vmem_limit_bytes=4 * 1024 * 1024),
        name="write",
    )(
        new_value,
        new_output,
        moved,
        copy_value.reshape(WIDE, COLS),
        copy_output.reshape(2 * CHIPS, COLS, 128),
    )


def solution(mesh):
    torus = Mesh(mesh.devices.reshape(4, 4, 2, 4), ("z", "y", "c", "x"))
    split = P(FS, "x")
    whole = P(FS, None)
    return jax.shard_map(
        shards,
        mesh=torus,
        in_specs=(
            split, split, P("x"), P("x"), whole, whole, split, whole, whole,
            split, P("x", FS), split, split, split, split,
        ),
        out_specs=(
            split, split, split, P(None, "x"), P("x", FS), split, split, P("x", None),
        ),
        check_vma=False,
    )
```

time: 257 us -> 95.5 us (0.37)
  waiting for transfers between devices: 157 us -> 0 us
  Pallas kernels: 0 us -> 94.8 us
  blocking collectives: 30.6 us -> 0 us
  matrix products: 17.3 us -> 0 us
  local copies, waits for them, and re-layouts: 17.3 us -> 0 us
  between operations: 16 us -> 0.65 us
  starting transfers between devices: 10.1 us -> 0 us
  other arithmetic: 8.61 us -> 0 us
    all_gather x3 -> x0, waiting for transfers between devices: 143 us -> none  [the longest x2 85.4 us: side_by_side(): lax.all_gather(both, axis, axis=dim, tiled=True)]
    pallas_call x0 -> x2, Pallas kernels: none -> 94.8 us  [the longest x1 91 us: shards(): pl.pallas_call(step_kernel, out_shape=(pltpu.VMEM((128, COLS), f32), pltp...]
    psum x4 -> x0, blocking collectives: 30.6 us -> none  [over_axes(): value = lax.psum(value, axis)]
    dot_general x6 -> x0, matrix products: 17.3 us -> none  [the longest x1 5.27 us: shards(): jnp.dot(cot_output, whole_output, preferred_element_type=jnp.float32)]
    all_to_all x2 -> x0, waiting for transfers between devices: 13.6 us -> none  [sent_and_summed(): lax.all_to_all(in_blocks(value, dim, devices), axis, 0, 0, tiled=True)]
    all_to_all x2 -> x0, starting transfers between devices: 9.94 us -> none  [sent_and_summed(): lax.all_to_all(in_blocks(value, dim, devices), axis, 0, 0, tiled=True)]
    unnamed x29 -> x0, local copies, waits for them, and re-layouts: 7.8 us -> none
    transpose x1 -> x0, local copies, waits for them, and re-layouts: 6.03 us -> none  [gather_turned(): outs.append(jnp.moveaxis(slab, 0, dim))]
  transfers between devices with their start and end apart: 5 -> 0, of which waited for: 5 -> 0; matrix products, arithmetic and copies ran while one was open for 6% -> 0% of each run, Pallas kernels for 0% -> 0%
where the time goes in v1:
time: 95.5 us; the launch traced here: 95.4 us
  Pallas kernels  94.8 us (99%)
    pallas_call x1, Pallas kernels, shards(): pl.pallas_call(step_kernel, out_shape=(pltpu.VMEM((128, COLS), f32), pltp...  91 us
    pallas_call x1, Pallas kernels, shards(): pl.pallas_call(write_kernel, out_shape=(jax.ShapeDtypeStruct((128, COLS),...  3.77 us

profile of v1, /device:TPU:1, one launch (start us, length us, event | category | flops | bytes accessed | tf_op | source)
XLA Modules:
  0.0 95.4 jit_solution(6314122280101369185)
XLA Ops:
  0.6 91.0 %step.1 = (f32[128,512]{1,0:T(8,128)S(1)}, f32[512,128]{1,0:T(8,128)S(1)}, f32[4,8,512]{2,1,0:T(8,128)S(1)}, bf16[16,2,128,512]{3,2,1,0:T(8,128)(2,1)S(1)}, bf16[16,2,512,128]{3,2,1,0:T(8,128)(2,1)S(1)}) custom-call(bf16[768,512]{1,0:T(8,128)(2,1)} %first_map.1, bf16[768,512]{1,0:T(8,128)(2,1)} %second_map.1, f32[4]{0:T(128)} %lambda_head.1, f32[512]{0:T(512)} %head_gain.1, ...), custom_call_target="tpu_custom_call" | custom-call | tf_op jit(solution)/shard_map/step/pallas_call | solution.py:374
  91.6 3.8 %write.1 = (f32[128,512]{1,0:T(8,128)}, f32[8,512]{1,0:T(8,128)}, f32[8,512]{1,0:T(8,128)}, bf16[4096,512]{1,0:T(8,128)(2,1)}, f32[512,128]{1,0:T(8,128)}, /*ind...) custom-call(f32[128,512]{1,0:T(8,128)S(1)} %get-tuple-element.13.new_value, ...), custom_call_target="tpu_custom_call" | custom-call | tf_op jit(solution)/shard_map/write/pallas_call | solution.py:419

commit v2 on v1

v2 whole, which is shorter than its diff:
```python
import math

import jax
import jax.numpy as jnp
from jax import lax
from jax.experimental import pallas as pl
from jax.experimental.pallas import tpu as pltpu
from jax.sharding import Mesh
from jax.sharding import PartitionSpec as P

MESH = pl.DeviceIdType.MESH
RANK = 256
HV = 2048
FS = ("z", "y", "c")

norm_epsilon = 1e-06
first_decay = 0.9
second_decay = 0.95
learn_rate = 0.1

ROWS = 768
WIDE = 4096
COLS = 512
HEADS_HERE = 4
CHIPS = 16

f32 = jnp.float32
bf16 = jnp.bfloat16


def step_kernel(
    first_map, second_map, lambda_head, head_gain, cot_output, layer_input, cot_values,
    factor_value, factor_output, weight_value, weight_output,
    first_value, second_value, first_output, second_output,
    new_value, new_output, moved, copy_value, copy_output,
    maps, lam, gain, wide, cots, heads, factors, weights_v, weights_o, moments,
    acc, lows, pair_in, summed, cross_in, squares, cross_sq, last_sq, low_all, ratios,
    load_sem, send_sem, recv_sem, pass_sem, pair_sem, cross_sem, sq_sem, low_sem, low_pass,
):
    z, y, c, x = (lax.axis_index(a) for a in ("z", "y", "c", "x"))
    own = 4 * z + y
    mine = 2 * own + c
    partner = (z, y, 1 - c, x)

    def near(z_by, y_by, c_by, x_by):
        return (
            lax.rem(z + z_by, 4), lax.rem(y + y_by, 4), lax.rem(c + c_by, 2), lax.rem(x + x_by, 4)
        )

    def at(dz, dy):
        return 4 * lax.rem(z + dz, 4) + lax.rem(y + dy, 4)

    def place(da, db, core):
        return at(da * core + db * (1 - core), da * (1 - core) + db * core)

    def chip_at(da, db):
        return near(da * c + db * (1 - c), da * (1 - c) + db * c, 0, 0)

    def remote(source, target, sent, arrived, device):
        return pltpu.make_async_remote_copy(
            source, target, sent, arrived, device_id=device, device_id_type=MESH
        )

    def arrive(block, semaphore):
        remote(block, block, send_sem.at[0, 0], semaphore, partner).wait_recv()

    def sent_off(block, semaphore):
        remote(block, block, semaphore, recv_sem.at[0, 0, 0], partner).wait_send()

    def load(k, source, target):
        copy = pltpu.make_async_copy(source, target, load_sem.at[k])
        copy.start()
        return copy

    own_factors = [
        load(0, factor_value, factors.at[0, mine]),
        load(1, factor_output, factors.at[1, mine]),
    ]
    barrier = pltpu.get_barrier_semaphore()
    greeted = [chip_at(1, 0), chip_at(3, 0), chip_at(0, 1), chip_at(0, 3), partner]
    greeted += [near(0, 0, dc, dx) for dx in (1, 2, 3) for dc in (0, 1)]
    for device in greeted:
        pl.semaphore_signal(barrier, inc=1, device_id=device, device_id_type=MESH)
    load_maps = [
        load(2, first_map, maps.at[0]),
        load(3, second_map, maps.at[1]),
        load(4, lambda_head, lam),
        load(5, head_gain, gain),
    ]
    load_wide = [load(6, layer_input, wide.at[0]), load(7, cot_output, wide.at[1])]
    load_moments = [
        load(8, first_value, moments.at[0, mine, 0]),
        load(9, second_value, moments.at[0, mine, 1]),
        load(10, first_output, moments.at[1, mine, 0]),
        load(11, second_output, moments.at[1, mine, 1]),
    ]
    load_rest = [
        load(12, cot_values, cots),
        load(13, weight_value, weights_v),
        load(14, weight_output, weights_o),
    ]
    for copy in own_factors:
        copy.wait()
    pl.semaphore_wait(barrier, len(greeted))

    LEVELS = (
        ((0, 0),),
        ((3, 0), (1, 0), (0, 3), (0, 1)),
        ((2, 0), (3, 3), (3, 1), (1, 3), (1, 1), (0, 2)),
        ((2, 3), (2, 1), (3, 2), (1, 2)),
        ((2, 2),),
    )

    class Gather:
        def __init__(self, stage, arrivals, halves):
            self.halves, self.counts = halves, [0, 0]
            self.sent = [send_sem.at[stage, h] for h in (0, 1)]
            self.arrived = recv_sem.at[arrivals]
            self.passed = pass_sem.at[stage]

        def fire(self, h, da, db, way):
            block = self.halves[h].at[2 * place(da, db, c) + c]
            if way == "d":
                level = min(da, 4 - da) + min(db, 4 - db)
                device, arrived = partner, self.passed.at[h, level]
            else:
                by = 1 if way[1] == "+" else 3
                if way[0] == "a":
                    device, da = chip_at(by, 0), (da - by) % 4
                else:
                    device, db = chip_at(0, by), (db - by) % 4
                arrived = self.arrived.at[h, 4 * da + db]
            remote(block, block, self.sent[h], arrived, device).start()
            self.counts[h] += 1

        def start(self, h):
            for way in ("b+", "b-", "a+", "a-", "d"):
                self.fire(h, 0, 0, way)

        def take(self, h, da, db):
            arrive(self.halves[h].at[2 * place(da, db, c) + c], self.arrived.at[h, 4 * da + db])
            if db == 0:
                if da == 3 and h == 0:
                    self.fire(h, da, db, "a+")
                if da == 1 and h == 1:
                    self.fire(h, da, db, "a-")
                self.fire(h, da, db, "b+")
                self.fire(h, da, db, "b-")
            if db == 3 and h == 0:
                self.fire(h, da, db, "b+")
            if db == 1 and h == 1:
                self.fire(h, da, db, "b-")
            self.fire(h, da, db, "d")

        def take_level(self, level, halves=(0, 1)):
            for h in halves:
                for da, db in LEVELS[level]:
                    self.take(h, da, db)

        def across(self, level):
            for h in (0, 1):
                arrive(self.halves[h].at[pl.ds(0, len(LEVELS[level]))], self.passed.at[h, level])

        def finish(self):
            for h in (0, 1):
                sent_off(self.halves[h].at[pl.ds(0, self.counts[h])], self.sent[h])

    gather = Gather(0, 0, (factors.at[0], factors.at[1]))
    gather.start(0)
    gather.start(1)

    for copy in load_maps:
        copy.wait()
    width = COLS // HEADS_HERE
    for h in range(HEADS_HERE):
        span = pl.ds(h * width, width)
        differ = maps[0, :, span].astype(f32) - lam[h] * maps[1, :, span].astype(f32)
        mean = jnp.sum(differ * differ, axis=-1, keepdims=True) * (1.0 / width)
        scaled = differ * lax.rsqrt(mean + norm_epsilon)
        heads[:, span] = (scaled * gain[span][None, :]).astype(bf16)

    def project(*chips, fresh=False):
        for m in (0, 1):
            left = [
                wide[m, :, pl.ds(pl.multiple_of(p * 256, 256), 256)]
                for p in chips
            ]
            right = [factors[m, pl.ds(2 * p, 2)].reshape(256, RANK) for p in chips]
            if len(chips) > 1:
                left, right = [jnp.concatenate(left, axis=1)], [jnp.concatenate(right, axis=0)]
            part = jnp.dot(left[0], right[0], preferred_element_type=f32)
            acc[m] = part if fresh else acc[m] + part

    gather.take_level(1)
    for copy in load_wide:
        copy.wait()
    gather.across(0)
    project(own, fresh=True)
    gather.take_level(2, (0,))
    gather.across(1)
    project(at(1, 0), at(3, 0))
    gather.take_level(2, (1,))
    project(at(0, 1), at(0, 3))
    gather.take_level(3, (0,))
    gather.across(2)
    project(at(2, 0), at(0, 2))
    gather.take_level(3, (1,))
    project(at(1, 1), at(3, 3))
    gather.take_level(4)
    for copy in load_moments:
        copy.wait()
    moment_gather = Gather(1, 1, (moments.at[0], moments.at[1]))
    moment_gather.start(0)
    moment_gather.start(1)
    project(at(1, 3), at(3, 1))
    gather.across(3)
    project(at(2, 1), at(2, 3))
    project(at(1, 2), at(3, 2))
    gather.across(4)
    project(at(2, 2))

    for copy in load_rest:
        copy.wait()
    pair = []
    for m in (0, 1):
        turned = acc[m].T
        high = turned.astype(bf16)
        low = (turned - high.astype(f32)).astype(bf16)
        right = (cots if m == 0 else heads)[...]
        product = jnp.dot(high, right, preferred_element_type=f32) + jnp.dot(
            low, right, preferred_element_type=f32
        )
        product = product.reshape(CHIPS, 2, 8, COLS)
        for core in (0, 1):
            lows[core, m] = product[:, core]
        copy = remote(
            lows.at[1 - c, m], pair_in.at[m], pair_sem.at[0, m], pair_sem.at[1, m], partner
        )
        copy.start()
        pair.append(copy)
    moment_gather.take_level(1)

    offsets = sorted(
        ((dz, dy) for dz in range(4) for dy in range(4) if (dz, dy) != (0, 0)),
        key=lambda o: -(min(o[0], 4 - o[0]) + min(o[1], 4 - o[1])),
    )
    for m in (0, 1):
        pair[m].wait_recv()
        summed[m] = lows[c, m] + pair_in[m]
        for k, (dz, dy) in enumerate(offsets):
            remote(
                summed.at[m, at(dz, dy)], cross_in.at[m, k], cross_sem.at[0, m], cross_sem.at[1, m],
                near(dz, dy, 0, 0),
            ).start()
    moment_gather.take_level(2)
    totals = []
    for m in (0, 1):
        arrive(cross_in.at[m], cross_sem.at[1, m])
        total = summed[m, own]
        for k in range(len(offsets)):
            total = total + cross_in[m, k]
        low_all[mine, m] = total
        totals.append(total)

    def fold(value):
        return sum(value[:, 128 * j : 128 * (j + 1)] for j in range(COLS // 128))

    squares[0] = fold(totals[0] * totals[0] + totals[1] * totals[1])
    for k, (dz, dy) in enumerate(offsets):
        remote(
            squares.at[0], cross_sq.at[k], sq_sem.at[0, 0], sq_sem.at[0, 1], near(dz, dy, 0, 0)
        ).start()
    block = low_all.at[mine]
    for k, (dz, dy) in enumerate(offsets):
        remote(block, block, low_sem.at[15], low_sem.at[k], near(dz, dy, 0, 0)).start()
    remote(block, block, low_pass.at[0], low_pass.at[1], partner).start()
    moment_gather.take_level(3)
    arrive(cross_sq, sq_sem.at[0, 1])
    plane = squares[0]
    for k in range(len(offsets)):
        plane = plane + cross_sq[k]
    squares[1] = plane
    for k, (dx, dc) in enumerate(((2, 1), (1, 1), (3, 1), (2, 0), (1, 0), (3, 0), (0, 1))):
        remote(
            squares.at[1], last_sq.at[k], sq_sem.at[1, 0], sq_sem.at[1, 1], near(0, 0, dc, dx)
        ).start()
    moment_gather.take_level(4)
    for k, (dz, dy) in reversed(list(enumerate(offsets))):
        block = low_all.at[2 * at((-dz) % 4, (-dy) % 4) + c]
        arrive(block, low_sem.at[k])
        remote(block, block, low_pass.at[0], low_pass.at[1], partner).start()
    arrive(last_sq, sq_sem.at[1, 1])
    whole = squares[1]
    for k in range(7):
        whole = whole + last_sq[k]
    square_sum = jnp.sum(jnp.sum(whole, axis=1, keepdims=True), axis=0, keepdims=True)
    clip = jnp.minimum(1.0, math.sqrt(RANK * HV) * lax.rsqrt(square_sum + norm_epsilon))
    for level in range(5):
        moment_gather.across(level)
    arrive(low_all.at[pl.ds(0, CHIPS)], low_pass.at[1])

    def moved_by(low, first_old, second_old):
        scaled = clip * low
        first_new = first_decay * first_old + (1.0 - first_decay) * scaled
        second_new = second_decay * second_old + (1.0 - second_decay) * scaled * scaled
        return first_new, second_new

    def added(m):
        step = 4
        for k in range(0, 2 * CHIPS, step):
            low = low_all[k : k + step, m].reshape(8 * step, COLS)
            first_old = moments[m, k : k + step, 0].reshape(8 * step, COLS)
            second_old = moments[m, k : k + step, 1].reshape(8 * step, COLS)
            first_new, second_new = moved_by(low, first_old, second_old)
            ratio = first_new * lax.rsqrt(second_new)
            high = ratio.astype(bf16)
            ratios[m, 0, 8 * k : 8 * (k + step)] = high
            ratios[m, 1, 8 * k : 8 * (k + step)] = (ratio - high.astype(f32)).astype(bf16)
        left = factors[m, mine]
        return jnp.dot(left, ratios[m, 0], preferred_element_type=f32) + jnp.dot(
            left, ratios[m, 1], preferred_element_type=f32
        )

    spread = Gather(2, 0, (copy_value, copy_output))
    fresh = weights_v[...] - learn_rate * added(0)
    copy_value[mine] = fresh.astype(bf16)
    spread.start(0)
    new_value[...] = fresh
    fresh = weights_o[...] - learn_rate * added(1).T
    copy_output[mine] = fresh.astype(bf16)
    spread.start(1)
    new_output[...] = fresh
    for m in (0, 1):
        first_new, second_new = moved_by(
            low_all[mine, m], moments[m, mine, 0], moments[m, mine, 1]
        )
        moved[2 * m] = first_new
        moved[2 * m + 1] = second_new
    gather.finish()
    moment_gather.finish()
    for copy in pair:
        copy.wait_send()
    for m in (0, 1):
        sent_off(cross_in.at[m], cross_sem.at[0, m])
    sent_off(cross_sq, sq_sem.at[0, 0])
    sent_off(last_sq, sq_sem.at[1, 0])
    sent_off(low_all.at[pl.ds(0, 15)], low_sem.at[15])
    sent_off(low_all.at[pl.ds(0, CHIPS)], low_pass.at[0])
    for level in (1, 2, 3, 4):
        spread.take_level(level)
    for level in range(5):
        spread.across(level)
    spread.finish()


def write_kernel(new_value, new_output, moved, copy_value, copy_output, *rest):
    outs, sem = rest[:8], rest[8]
    new_v, first_v, second_v, copy_v, new_o, first_o, second_o, copy_o = outs
    pairs = [(copy_value, copy_v)]
    pairs += [
        (copy_output.at[k], copy_o.at[:, pl.ds(128 * k, 128)]) for k in range(copy_output.shape[0])
    ]
    pairs += [(new_value, new_v), (new_output, new_o)]
    pairs += [(moved.at[k], out) for k, out in enumerate((first_v, second_v, first_o, second_o))]
    copies = [pltpu.make_async_copy(s, t, sem.at[k]) for k, (s, t) in enumerate(pairs)]
    for copy in copies:
        copy.start()
    for copy in copies:
        copy.wait()


def shards(*args):
    any_space = pl.BlockSpec(memory_space=pltpu.HBM)
    vmem = pl.BlockSpec(memory_space=pltpu.VMEM)
    dma = pltpu.SemaphoreType.DMA
    new_value, new_output, moved, copy_value, copy_output = pl.pallas_call(
        step_kernel,
        out_shape=(
            pltpu.VMEM((128, COLS), f32),
            pltpu.VMEM((COLS, 128), f32),
            pltpu.VMEM((4, 8, COLS), f32),
            pltpu.VMEM((2 * CHIPS, 128, COLS), bf16),
            pltpu.VMEM((2 * CHIPS, COLS, 128), bf16),
        ),
        in_specs=[any_space] * 15,
        out_specs=(vmem,) * 5,
        scratch_shapes=[
            pltpu.VMEM((2, ROWS, COLS), bf16),
            pltpu.SMEM((HEADS_HERE,), f32),
            pltpu.VMEM((COLS,), f32),
            pltpu.VMEM((2, ROWS, WIDE), bf16),
            pltpu.VMEM((ROWS, COLS), bf16),
            pltpu.VMEM((ROWS, COLS), bf16),
            pltpu.VMEM((2, 2 * CHIPS, 128, RANK), bf16),
            pltpu.VMEM((128, COLS), f32),
            pltpu.VMEM((COLS, 128), f32),
            pltpu.VMEM((2, 2 * CHIPS, 2, 8, COLS), f32),
            pltpu.VMEM((2, ROWS, RANK), f32),
            pltpu.VMEM((2, 2, CHIPS, 8, COLS), f32),
            pltpu.VMEM((2, CHIPS, 8, COLS), f32),
            pltpu.VMEM((2, CHIPS, 8, COLS), f32),
            pltpu.VMEM((2, 15, 8, COLS), f32),
            pltpu.VMEM((2, 8, 128), f32),
            pltpu.VMEM((15, 8, 128), f32),
            pltpu.VMEM((7, 8, 128), f32),
            pltpu.VMEM((2 * CHIPS, 2, 8, COLS), f32),
            pltpu.VMEM((2, 2, RANK, COLS), bf16),
            dma((15,)),
            dma((3, 2)),
            dma((2, 2, 16)),
            dma((3, 2, 5)),
            dma((2, 2)),
            dma((2, 2)),
            dma((2, 2)),
            dma((16,)),
            dma((2,)),
        ],
        compiler_params=pltpu.CompilerParams(
            collective_id=0, has_side_effects=True, vmem_limit_bytes=46 * 1024 * 1024
        ),
        name="step",
    )(*args)
    return pl.pallas_call(
        write_kernel,
        out_shape=(
            jax.ShapeDtypeStruct((128, COLS), f32),
            jax.ShapeDtypeStruct((8, COLS), f32),
            jax.ShapeDtypeStruct((8, COLS), f32),
            jax.ShapeDtypeStruct((WIDE, COLS), bf16),
            jax.ShapeDtypeStruct((COLS, 128), f32),
            jax.ShapeDtypeStruct((8, COLS), f32),
            jax.ShapeDtypeStruct((8, COLS), f32),
            jax.ShapeDtypeStruct((COLS, WIDE), bf16),
        ),
        in_specs=[vmem] * 5,
        out_specs=(any_space,) * 8,
        scratch_shapes=[dma((2 * CHIPS + 7,))],
        compiler_params=pltpu.CompilerParams(vmem_limit_bytes=4 * 1024 * 1024),
        name="write",
    )(
        new_value,
        new_output,
        moved,
        copy_value.reshape(WIDE, COLS),
        copy_output,
    )


def solution(mesh):
    torus = Mesh(mesh.devices.reshape(4, 4, 2, 4), ("z", "y", "c", "x"))
    split = P(FS, "x")
    whole = P(FS, None)
    return jax.shard_map(
        shards,
        mesh=torus,
        in_specs=(
            split, split, P("x"), P("x"), whole, whole, split, whole, whole,
            split, P("x", FS), split, split, split, split,
        ),
        out_specs=(
            split, split, split, P(None, "x"), P("x", FS), split, split, P("x", None),
        ),
        check_vma=False,
    )
```

time: 95.5 us -> 83.8 us (0.88)
  Pallas kernels: 94.8 us -> 83 us
    pallas_call x1, Pallas kernels: 91 us -> 79.3 us  [shards(): pl.pallas_call(step_kernel, out_shape=(pltpu.VMEM((128, COLS), f32), pltp...]
where the time goes in v2:
time: 83.8 us; the launch traced here: 83.7 us
  Pallas kernels  83 us (99%)
    pallas_call x1, Pallas kernels, shards(): pl.pallas_call(step_kernel, out_shape=(pltpu.VMEM((128, COLS), f32), pltp...  79.3 us
    pallas_call x1, Pallas kernels, shards(): pl.pallas_call(write_kernel, out_shape=(jax.ShapeDtypeStruct((128, COLS),...  3.77 us

profile of v2, /device:TPU:1, one launch (start us, length us, event | category | flops | bytes accessed | tf_op | source)
XLA Modules:
  0.0 83.7 jit_solution(15379750601897760795)
XLA Ops:
  0.6 79.3 %step.1 = (f32[128,512]{1,0:T(8,128)S(1)}, f32[512,128]{1,0:T(8,128)S(1)}, f32[4,8,512]{2,1,0:T(8,128)S(1)}, bf16[32,128,512]{2,1,0:T(8,128)(2,1)S(1)}, bf16[32,512,128]{2,1,0:T(8,128)(2,1)S(1)}) custom-call(bf16[768,512]{1,0:T(8,128)(2,1)} %first_map.1, bf16[768,512]{1,0:T(8,128)(2,1)} %second_map.1, f32[4]{0:T(128)} %lambda_head.1, f32[512]{0:T(512)} %head_gain.1, ...), custom_call_target="tpu_custom_call" | custom-call | tf_op jit(solution)/shard_map/step/pallas_call | solution.py:376
  79.9 3.8 %write.1 = (f32[128,512]{1,0:T(8,128)}, f32[8,512]{1,0:T(8,128)}, f32[8,512]{1,0:T(8,128)}, bf16[4096,512]{1,0:T(8,128)(2,1)}, f32[512,128]{1,0:T(8,128)}, /*ind...) custom-call(f32[128,512]{1,0:T(8,128)S(1)} %get-tuple-element.13.new_value, ...), custom_call_target="tpu_custom_call" | custom-call | tf_op jit(solution)/shard_map/write/pallas_call | solution.py:423

commit v3 on v2

v3 whole, which is shorter than its diff:
```python
import math

import jax
import jax.numpy as jnp
from jax import lax
from jax.experimental import pallas as pl
from jax.experimental.pallas import tpu as pltpu
from jax.sharding import Mesh
from jax.sharding import PartitionSpec as P

MESH = pl.DeviceIdType.MESH
RANK = 256
HV = 2048
FS = ("z", "y", "c")

norm_epsilon = 1e-06
first_decay = 0.9
second_decay = 0.95
learn_rate = 0.1

ROWS = 768
WIDE = 4096
COLS = 512
HEADS_HERE = 4
CHIPS = 16
LANES = 128

f32 = jnp.float32
bf16 = jnp.bfloat16

LEVELS = (
    ((0, 0),),
    ((3, 0), (1, 0), (0, 3), (0, 1)),
    ((2, 0), (3, 3), (3, 1), (1, 3), (1, 1), (0, 2)),
    ((2, 3), (2, 1), (3, 2), (1, 2)),
    ((2, 2),),
)


def step_kernel(
    first_map, second_map, lambda_head, head_gain, cot_output, layer_input, cot_values,
    factor_value, factor_output, weight_value, weight_output,
    first_value, second_value, first_output, second_output,
    new_weights, moved, copies,
    maps, lam, gain, wide, rights, right_in, factors, weights, moments,
    acc, turned, summed, cross_in, squares, cross_sq, last_sq, low_all, ratios, added, back, back_moved,
    load_sem, out_sem, in_sem, send_sem, recv_sem, pass_sem, cross_sem, sq_sem, low_sem,
):
    z, y, c, x = (lax.axis_index(a) for a in ("z", "y", "c", "x"))
    own = 4 * z + y
    mine = 2 * own + c
    partner = (z, y, 1 - c, x)

    def near(z_by, y_by, c_by, x_by):
        return (
            lax.rem(z + z_by, 4), lax.rem(y + y_by, 4), lax.rem(c + c_by, 2), lax.rem(x + x_by, 4)
        )

    def at(dz, dy):
        return 4 * lax.rem(z + dz, 4) + lax.rem(y + dy, 4)

    def place(da, db):
        return at(da * c + db * (1 - c), da * (1 - c) + db * c)

    def chip_at(da, db):
        return near(da * c + db * (1 - c), da * (1 - c) + db * c, 0, 0)

    def remote(source, target, sent, arrived, device):
        return pltpu.make_async_remote_copy(
            source, target, sent, arrived, device_id=device, device_id_type=MESH
        )

    def arrive(block, semaphore):
        remote(block, block, out_sem.at[0], semaphore, partner).wait_recv()

    def sent_off(block, semaphore):
        remote(block, block, semaphore, in_sem.at[0], partner).wait_send()

    def load(k, source, target):
        copy = pltpu.make_async_copy(source, target, load_sem.at[k])
        copy.start()
        return copy

    def loaded(k, target):
        pltpu.make_async_copy(target, target, load_sem.at[k]).wait()

    value_args = (factor_value, first_value, second_value, layer_input)
    output_args = (factor_output, first_output, second_output, cot_output)

    def columns(ref, j):
        return ref.at[:, pl.ds(LANES * j, LANES)]

    def rows(ref, j):
        return ref.at[pl.ds(LANES * j, LANES)]

    def load_first(args):
        load(0, args[0], factors.at[mine])

    def load_later(args, weight, pieces):
        load(1, args[3], wide.at[0])
        load(2, args[1], moments.at[mine, 0])
        load(2, args[2], moments.at[mine, 1])
        for j in range(4):
            load(3, pieces(weight, j), rows(weights.at[c], j))

    pl.when(c == 0)(lambda: load_first(value_args))
    pl.when(c == 1)(lambda: load_first(output_args))
    barrier = pltpu.get_barrier_semaphore()
    greeted = [chip_at(1, 0), chip_at(3, 0), chip_at(0, 1), chip_at(0, 3), partner]
    greeted += [near(0, 0, dc, dx) for dx in (1, 2, 3) for dc in (0, 1)]
    for device in greeted:
        pl.semaphore_signal(barrier, inc=1, device_id=device, device_id_type=MESH)
    load_maps = [
        load(4, first_map, maps.at[0]),
        load(5, second_map, maps.at[1]),
        load(6, lambda_head, lam),
        load(7, head_gain, gain),
    ]
    pl.when(c == 0)(lambda: load_later(value_args, weight_value, columns))
    pl.when(c == 1)(lambda: load_later(output_args, weight_output, rows))
    load(8, cot_values, rights.at[0])
    pl.semaphore_wait(barrier, len(greeted))

    def hand(k, source, target):
        remote(source, target, out_sem.at[k], in_sem.at[k], partner).start()

    def hand_later(args, weight, pieces):
        hand(1, args[3], wide.at[1])
        hand(2, args[1], moments.at[mine, 0])
        hand(2, args[2], moments.at[mine, 1])
        for j in range(4):
            hand(3, pieces(weight, j), rows(weights.at[c], j))

    pl.when(c == 0)(lambda: hand(0, factor_output, factors.at[mine]))
    pl.when(c == 1)(lambda: hand(0, factor_value, factors.at[mine]))

    class Gather:
        def __init__(self, stage, arrivals, blocks, passed=None):
            self.blocks, self.passed, self.sent = blocks, passed, send_sem.at[stage]
            self.counts = [0, 0]
            self.arrived = recv_sem.at[arrivals]

        def block(self, g, da, db):
            return self.blocks.at[2 * place(da, db) + (c if g == 0 else 1 - c)]

        def fire(self, g, da, db, *ways):
            block = self.block(g, da, db)
            for way in ways:
                ra, rb = da, db
                by = 1 if way[1] == "+" else 3
                if way[0] == "a":
                    device, ra = chip_at(by, 0), (da - by) % 4
                else:
                    device, rb = chip_at(0, by), (db - by) % 4
                remote(
                    block, block, self.sent.at[g], self.arrived.at[g, 4 * ra + rb], device
                ).start()
                self.counts[g] += 1
            if self.passed is not None:
                level = min(da, 4 - da) + min(db, 4 - db)
                remote(block, block, self.sent.at[g], self.passed.at[level], partner).start()
                self.counts[g] += 1

        def start(self, g):
            self.fire(g, 0, 0, "b+", "b-", "a+", "a-")

        def take(self, g, da, db):
            arrive(self.block(g, da, db), self.arrived.at[g, 4 * da + db])
            ways = []
            if db == 0:
                if da == (3 if g == 0 else 1):
                    ways.append("a+" if g == 0 else "a-")
                ways += ["b+", "b-"]
            elif db == (3 if (da in (0, 1)) == (g == 0) else 1):
                ways.append("b+" if db == 3 else "b-")
            self.fire(g, da, db, *ways)

        def take_level(self, level, parts=(0, 1)):
            for g in parts:
                for da, db in LEVELS[level]:
                    self.take(g, da, db)

        def finish(self):
            for g in (0, 1):
                sent_off(self.blocks.at[pl.ds(0, self.counts[g])], self.sent.at[g])

    loaded(0, factors.at[mine])
    gather = Gather(0, 0, factors)
    gather.start(0)
    pl.when(c == 0)(lambda: hand_later(output_args, weight_output, rows))
    pl.when(c == 1)(lambda: hand_later(value_args, weight_value, columns))
    for copy in load_maps:
        copy.wait()
    width = COLS // HEADS_HERE
    for h in range(HEADS_HERE):
        span = pl.ds(h * width, width)
        differ = maps[0, :, span].astype(f32) - lam[h] * maps[1, :, span].astype(f32)
        mean = jnp.sum(differ * differ, axis=-1, keepdims=True) * (1.0 / width)
        scaled = differ * lax.rsqrt(mean + norm_epsilon)
        rights[1, :, span] = (scaled * gain[span][None, :]).astype(bf16)
    arrive(factors.at[mine], in_sem.at[0])
    gather.start(1)
    loaded(8, rights.at[0])
    hand(4, rights.at[1 - c], right_in)

    def project(t, *chips, fresh=False):
        left = [wide[t, :, pl.ds(pl.multiple_of(p * 256, 256), 256)] for p in chips]
        right = [factors[pl.ds(2 * p, 2)].reshape(256, RANK) for p in chips]
        if len(chips) > 1:
            left, right = [jnp.concatenate(left, axis=1)], [jnp.concatenate(right, axis=0)]
        part = jnp.dot(left[0], right[0], preferred_element_type=f32)
        acc[t] = part if fresh else acc[t] + part

    PAIRS = (
        None,
        (((1, 0), (3, 0)), ((0, 1), (0, 3))),
        (((2, 0), (0, 2)), ((1, 1), (3, 3)), ((1, 3), (3, 1))),
        (((2, 1), (2, 3)), ((1, 2), (3, 2))),
    )

    def project_pairs(t, level, *which):
        for k in which:
            (z0, y0), (z1, y1) = PAIRS[level][k]
            project(t, at(z0, y0), at(z1, y1))

    gather.take_level(1)
    loaded(1, wide.at[0])
    project(0, own, fresh=True)
    gather.take_level(2, (0,))
    project_pairs(0, 1, 0)
    gather.take_level(2, (1,))
    project_pairs(0, 1, 1)
    gather.take_level(3, (0,))
    arrive(wide.at[1], in_sem.at[1])
    project(1, own, fresh=True)
    project_pairs(1, 1, 0)
    loaded(2, moments.at[mine])
    arrive(moments.at[mine], in_sem.at[2])
    moment_gather = Gather(1, 1, moments)
    moment_gather.start(0)
    moment_gather.start(1)
    gather.take_level(3, (1,))
    project_pairs(1, 1, 1)
    project_pairs(0, 2, 0, 1, 2)
    project_pairs(1, 2, 0)
    project_pairs(1, 2, 1, 2)
    project_pairs(0, 3, 0, 1)
    gather.take_level(4)
    moment_gather.take_level(1)
    project_pairs(1, 3, 0, 1)
    for t in (0, 1):
        project(t, at(2, 2))
    arrive(right_in, in_sem.at[4])
    product = None
    for t in (0, 1):
        flat = acc[t].T
        high = flat.astype(bf16)
        turned[t, :RANK] = high
        turned[t, RANK:] = (flat - high.astype(f32)).astype(bf16)
        right = rights[c] if t == 0 else right_in[...]
        part = jnp.dot(turned[t], right, preferred_element_type=f32)
        product = part if t == 0 else product + part
    summed[...] = (product[:RANK] + product[RANK:]).reshape(CHIPS, 16, COLS)

    offsets = sorted(
        ((dz, dy) for dz in range(4) for dy in range(4) if (dz, dy) != (0, 0)),
        key=lambda o: -(min(o[0], 4 - o[0]) + min(o[1], 4 - o[1])),
    )
    for k, (dz, dy) in enumerate(offsets):
        remote(
            summed.at[at(dz, dy)], cross_in.at[k], cross_sem.at[0], cross_sem.at[1],
            near(dz, dy, 0, 0),
        ).start()
    arrive(cross_in, cross_sem.at[1])
    total = summed[own]
    for k in range(len(offsets)):
        total = total + cross_in[k]
    low_all[own] = total

    def fold(value):
        value = value[:8] + value[8:]
        return sum(value[:, LANES * j : LANES * (j + 1)] for j in range(COLS // LANES))

    squares[0] = fold(total * total)
    for k, (dz, dy) in enumerate(offsets):
        remote(
            squares.at[0], cross_sq.at[k], sq_sem.at[0, 0], sq_sem.at[0, 1], near(dz, dy, 0, 0)
        ).start()
    def send_low(block, way):
        for by in (2, 1, 3):
            device = chip_at(by, 0) if way == 0 else chip_at(0, by)
            remote(block, block, low_sem.at[way, 0], low_sem.at[way, 1], device).start()

    send_low(low_all.at[own], 0)
    send_low(low_all.at[own], 1)
    moment_gather.take_level(2)
    arrive(low_all.at[pl.ds(0, 3)], low_sem.at[0, 1])
    for k in (2, 1, 3):
        send_low(low_all.at[place(k, 0)], 1)
    arrive(cross_sq, sq_sem.at[0, 1])
    plane = squares[0]
    for k in range(len(offsets)):
        plane = plane + cross_sq[k]
    squares[1] = plane
    for k, (dx, dc) in enumerate(((2, 1), (1, 1), (3, 1), (2, 0), (1, 0), (3, 0), (0, 1))):
        remote(
            squares.at[1], last_sq.at[k], sq_sem.at[1, 0], sq_sem.at[1, 1], near(0, 0, dc, dx)
        ).start()
    moment_gather.take_level(3)
    arrive(weights.at[0], in_sem.at[3])
    loaded(3, weights.at[0])
    arrive(low_all.at[pl.ds(0, 12)], low_sem.at[1, 1])
    arrive(last_sq, sq_sem.at[1, 1])
    whole = squares[1]
    for k in range(7):
        whole = whole + last_sq[k]
    square_sum = jnp.sum(jnp.sum(whole, axis=1, keepdims=True), axis=0, keepdims=True)
    clip = jnp.minimum(1.0, math.sqrt(RANK * HV) * lax.rsqrt(square_sum + norm_epsilon))

    moment_gather.take_level(4)
    def moved_by(low, first_old, second_old):
        scaled = clip * low
        first_new = first_decay * first_old + (1.0 - first_decay) * scaled
        second_new = second_decay * second_old + (1.0 - second_decay) * scaled * scaled
        return first_new, second_new

    step = 2
    for k in range(0, CHIPS, step):
        low = low_all[k : k + step].reshape(16 * step, COLS)
        first_old = moments[2 * k : 2 * (k + step), 0].reshape(16 * step, COLS)
        second_old = moments[2 * k : 2 * (k + step), 1].reshape(16 * step, COLS)
        first_new, second_new = moved_by(low, first_old, second_old)
        ratio = first_new * lax.rsqrt(second_new)
        high = ratio.astype(bf16)
        ratios[0, 16 * k : 16 * (k + step)] = high
        ratios[1, 16 * k : 16 * (k + step)] = (ratio - high.astype(f32)).astype(bf16)
    left = factors[pl.ds(2 * own, 2)].reshape(256, RANK)
    added[...] = (
        jnp.dot(left, ratios[0], preferred_element_type=f32)
        + jnp.dot(left, ratios[1], preferred_element_type=f32)
    ).reshape(2, LANES, COLS)

    spread = Gather(2, 0, copies.at[c], pass_sem)
    for g in (0, 1):
        core = c if g == 0 else 1 - c
        for j in range(4):
            span = pl.ds(LANES * j, LANES)
            update = added[core, :, span]
            update = jnp.where(c == 0, update, update.T)
            fresh = weights[core, span] - learn_rate * update
            copies[c, 2 * own + core, span] = fresh.astype(bf16)
            if g == 0:
                new_weights[c, span] = fresh
            else:
                back[span] = fresh
        spread.start(g)
    for g in (0, 1):
        core = c if g == 0 else 1 - c
        first_new, second_new = moved_by(
            low_all[own, pl.ds(8 * core, 8)], moments[2 * own + core, 0], moments[2 * own + core, 1]
        )
        target = moved.at[c] if g == 0 else back_moved
        target[0] = first_new
        target[1] = second_new
    hand(5, back, new_weights.at[c])
    hand(6, back_moved, moved.at[c])
    gather.finish()
    moment_gather.finish()
    sent_off(factors.at[0], out_sem.at[0])
    sent_off(wide.at[0], out_sem.at[1])
    sent_off(moments.at[0], out_sem.at[2])
    sent_off(weights.at[0], out_sem.at[3])
    sent_off(right_in, out_sem.at[4])
    sent_off(cross_in, cross_sem.at[0])
    sent_off(cross_sq, sq_sem.at[0, 0])
    sent_off(last_sq, sq_sem.at[1, 0])
    sent_off(low_all.at[pl.ds(0, 3)], low_sem.at[0, 0])
    sent_off(low_all.at[pl.ds(0, 12)], low_sem.at[1, 0])
    for level in (1, 2, 3, 4):
        spread.take_level(level)
    sent_off(back, out_sem.at[5])
    sent_off(back_moved, out_sem.at[6])
    arrive(back, in_sem.at[5])
    arrive(back_moved, in_sem.at[6])
    for level in range(5):
        arrive(copies.at[0, pl.ds(0, 2 * len(LEVELS[level]))], pass_sem.at[level])
    spread.finish()


def write_kernel(new_weights, moved, copies, *rest):
    outs, sem = rest[:8], rest[8]
    new_v, first_v, second_v, copy_v, new_o, first_o, second_o, copy_o = outs
    pairs = []
    for j in range(4):
        span = pl.ds(LANES * j, LANES)
        pairs.append((copies.at[0, :, span], copy_v.at[:, :, span]))
        pairs.append((new_weights.at[0, span], new_v.at[:, span]))
    for k in range(2 * CHIPS):
        pairs.append((copies.at[1, k], copy_o.at[:, pl.ds(LANES * k, LANES)]))
    pairs += [
        (new_weights.at[1], new_o),
        (moved.at[0, 0], first_v),
        (moved.at[0, 1], second_v),
        (moved.at[1, 0], first_o),
        (moved.at[1, 1], second_o),
    ]
    started = [pltpu.make_async_copy(s, t, sem.at[k]) for k, (s, t) in enumerate(pairs)]
    for copy in started:
        copy.start()
    for copy in started:
        copy.wait()


def shards(*args):
    hbm = pl.BlockSpec(memory_space=pltpu.HBM)
    vmem = pl.BlockSpec(memory_space=pltpu.VMEM)
    dma = pltpu.SemaphoreType.DMA
    passed = pl.pallas_call(
        step_kernel,
        out_shape=(
            pltpu.VMEM((2, COLS, LANES), f32),
            pltpu.VMEM((2, 2, 8, COLS), f32),
            pltpu.VMEM((2, 2 * CHIPS, COLS, LANES), bf16),
        ),
        in_specs=[hbm] * 15,
        out_specs=(vmem,) * 3,
        scratch_shapes=[
            pltpu.VMEM((2, ROWS, COLS), bf16),
            pltpu.SMEM((HEADS_HERE,), f32),
            pltpu.VMEM((COLS,), f32),
            pltpu.VMEM((2, ROWS, WIDE), bf16),
            pltpu.VMEM((2, ROWS, COLS), bf16),
            pltpu.VMEM((ROWS, COLS), bf16),
            pltpu.VMEM((2 * CHIPS, LANES, RANK), bf16),
            pltpu.VMEM((2, COLS, LANES), f32),
            pltpu.VMEM((2 * CHIPS, 2, 8, COLS), f32),
            pltpu.VMEM((2, ROWS, RANK), f32),
            pltpu.VMEM((2, 2 * RANK, ROWS), bf16),
            pltpu.VMEM((CHIPS, 16, COLS), f32),
            pltpu.VMEM((CHIPS - 1, 16, COLS), f32),
            pltpu.VMEM((2, 8, LANES), f32),
            pltpu.VMEM((CHIPS - 1, 8, LANES), f32),
            pltpu.VMEM((7, 8, LANES), f32),
            pltpu.VMEM((CHIPS, 16, COLS), f32),
            pltpu.VMEM((2, RANK, COLS), bf16),
            pltpu.VMEM((2, LANES, COLS), f32),
            pltpu.VMEM((COLS, LANES), f32),
            pltpu.VMEM((2, 8, COLS), f32),
            dma((9,)),
            dma((7,)),
            dma((7,)),
            dma((3, 2)),
            dma((2, 2, 16)),
            dma((5,)),
            dma((2,)),
            dma((2, 2)),
            dma((2, 2)),
        ],
        compiler_params=pltpu.CompilerParams(
            collective_id=0, has_side_effects=True, vmem_limit_bytes=46 * 1024 * 1024
        ),
        name="step",
    )(*args)
    outs = pl.pallas_call(
        write_kernel,
        out_shape=(
            jax.ShapeDtypeStruct((LANES, COLS), f32),
            jax.ShapeDtypeStruct((8, COLS), f32),
            jax.ShapeDtypeStruct((8, COLS), f32),
            jax.ShapeDtypeStruct((2 * CHIPS, LANES, COLS), bf16),
            jax.ShapeDtypeStruct((COLS, LANES), f32),
            jax.ShapeDtypeStruct((8, COLS), f32),
            jax.ShapeDtypeStruct((8, COLS), f32),
            jax.ShapeDtypeStruct((COLS, WIDE), bf16),
        ),
        in_specs=[vmem] * 3,
        out_specs=(hbm,) * 8,
        scratch_shapes=[dma((2 * CHIPS + 13,))],
        compiler_params=pltpu.CompilerParams(vmem_limit_bytes=4 * 1024 * 1024),
        name="write",
    )(*passed)
    return (*outs[:3], outs[3].reshape(WIDE, COLS), *outs[4:])


def solution(mesh):
    torus = Mesh(mesh.devices.reshape(4, 4, 2, 4), ("z", "y", "c", "x"))
    split = P(FS, "x")
    whole = P(FS, None)
    return jax.shard_map(
        shards,
        mesh=torus,
        in_specs=(
            split, split, P("x"), P("x"), whole, whole, split, whole, whole,
            split, P("x", FS), split, split, split, split,
        ),
        out_specs=(
            split, split, split, P(None, "x"), P("x", FS), split, split, P("x", None),
        ),
        check_vma=False,
    )
```

time: 83.8 us -> 77.5 us (0.925)
  Pallas kernels: 83 us -> 76.8 us
    pallas_call x2, Pallas kernels: 83 us -> 76.8 us  [the longest x1 72.9 us: shards(): pl.pallas_call(step_kernel, out_shape=(pltpu.VMEM((2, COLS, LANES), f32),...]
where the time goes in v3:
time: 77.5 us; the launch traced here: 77.4 us
  Pallas kernels  76.8 us (99%)
    pallas_call x1, Pallas kernels, shards(): pl.pallas_call(step_kernel, out_shape=(pltpu.VMEM((2, COLS, LANES), f32),...  72.9 us
    pallas_call x1, Pallas kernels, shards(): pl.pallas_call(write_kernel, out_shape=(jax.ShapeDtypeStruct((LANES, COLS...  3.83 us

profile of v3, /device:TPU:1, one launch (start us, length us, event | category | flops | bytes accessed | tf_op | source)
XLA Modules:
  0.0 77.4 jit_solution(18275030573505050658)
XLA Ops:
  0.6 72.9 %step.1 = (f32[2,512,128]{2,1,0:T(8,128)S(1)}, f32[2,2,8,512]{3,2,1,0:T(8,128)S(1)}, bf16[2,32,512,128]{3,2,1,0:T(8,128)(2,1)S(1)}) custom-call(bf16[768,512]{1,0:T(8,128)(2,1)} %first_map.1, bf16[768,512]{1,0:T(8,128)(2,1)} %second_map.1, f32[4]{0:T(128)} %lambda_head.1, f32[512]{0:T(512)} %head_gain.1, bf16[768,4096]{1,0:T(8,128)(2,1)} %cot_output.1, ...), custom_call_target="tpu_custom_call" | custom-call | tf_op jit(solution)/shard_map/step/pallas_call | solution.py:418
  73.6 3.8 %write.1 = (f32[128,512]{1,0:T(8,128)}, f32[8,512]{1,0:T(8,128)}, f32[8,512]{1,0:T(8,128)}, bf16[32,128,512]{2,1,0:T(8,128)(2,1)}, f32[512,128]{1,0:T(8,128)}, /...) custom-call(f32[2,512,128]{2,1,0:T(8,128)S(1)} %get-tuple-element.19.new_weights, ...), custom_call_target="tpu_custom_call" | custom-call | tf_op jit(solution)/shard_map/write/pallas_call | solution.py:464

commit v4 on v3

--- a/solution.py
+++ b/solution.py
@@ -35,6 +35,14 @@
     ((2, 3), (2, 1), (3, 2), (1, 2)),
     ((2, 2),),
 )
+GROUPS = (
+    (),
+    (((3, 0),), ((1, 0),), ((0, 3), (0, 1))),
+    (((2, 0),), ((3, 3), (3, 1), (1, 3), (1, 1), (0, 2))),
+    (((2, 3), (2, 1)), ((3, 2), (1, 2))),
+    (((2, 2),),),
+)
+GROUP_OF = {p: k for k, group in enumerate(sum(GROUPS, ())) for p in group}
 
 
 def step_kernel(
@@ -44,7 +52,7 @@
     new_weights, moved, copies,
     maps, lam, gain, wide, rights, right_in, factors, weights, moments,
     acc, turned, summed, cross_in, squares, cross_sq, last_sq, low_all, ratios, added, back, back_moved,
-    load_sem, out_sem, in_sem, send_sem, recv_sem, pass_sem, cross_sem, sq_sem, low_sem,
+    load_sem, out_sem, in_sem, send_sem, recv_sem, moment_sem, pass_sem, cross_sem, sq_sem, low_sem,
 ):
     z, y, c, x = (lax.axis_index(a) for a in ("z", "y", "c", "x"))
     own = 4 * z + y
@@ -79,7 +87,6 @@
     def load(k, source, target):
         copy = pltpu.make_async_copy(source, target, load_sem.at[k])
         copy.start()
-        return copy
 
     def loaded(k, target):
         pltpu.make_async_copy(target, target, load_sem.at[k]).wait()
@@ -110,15 +117,13 @@
     greeted += [near(0, 0, dc, dx) for dx in (1, 2, 3) for dc in (0, 1)]
     for device in greeted:
         pl.semaphore_signal(barrier, inc=1, device_id=device, device_id_type=MESH)
-    load_maps = [
-        load(4, first_map, maps.at[0]),
-        load(5, second_map, maps.at[1]),
-        load(6, lambda_head, lam),
-        load(7, head_gain, gain),
-    ]
+    load(4, first_map, maps.at[0])
+    load(4, second_map, maps.at[1])
+    load(5, lambda_head, lam)
+    load(6, head_gain, gain)
     pl.when(c == 0)(lambda: load_later(value_args, weight_value, columns))
     pl.when(c == 1)(lambda: load_later(output_args, weight_output, rows))
-    load(8, cot_values, rights.at[0])
+    load(7, cot_values, rights.at[0])
     pl.semaphore_wait(barrier, len(greeted))
 
     def hand(k, source, target):
@@ -135,16 +140,19 @@
     pl.when(c == 1)(lambda: hand(0, factor_value, factors.at[mine]))
 
     class Gather:
-        def __init__(self, stage, arrivals, blocks, passed=None):
+        def __init__(self, stage, arrived, blocks, parts, passed=None):
             self.blocks, self.passed, self.sent = blocks, passed, send_sem.at[stage]
+            self.parts, self.size = parts, blocks.shape[1] // parts
+            self.pieces = [(g, s) for g in (0, 1) for s in range(parts)]
             self.counts = [0, 0]
-            self.arrived = recv_sem.at[arrivals]
-
-        def block(self, g, da, db):
-            return self.blocks.at[2 * place(da, db) + (c if g == 0 else 1 - c)]
-
-        def fire(self, g, da, db, *ways):
-            block = self.block(g, da, db)
+            self.arrived = arrived
+
+        def piece(self, g, s, da, db):
+            block = self.blocks.at[2 * place(da, db) + (c if g == 0 else 1 - c)]
+            return block.at[pl.ds(self.size * s, self.size)]
+
+        def fire(self, g, s, da, db, *ways):
+            block = self.piece(g, s, da, db)
             for way in ways:
                 ra, rb = da, db
                 by = 1 if way[1] == "+" else 3
@@ -152,45 +160,49 @@
                     device, ra = chip_at(by, 0), (da - by) % 4
                 else:
                     device, rb = chip_at(0, by), (db - by) % 4
-                remote(
-                    block, block, self.sent.at[g], self.arrived.at[g, 4 * ra + rb], device
-                ).start()
+                arrived = self.arrived.at[self.parts * g + s, GROUP_OF[ra, rb]]
+                remote(block, block, self.sent.at[g], arrived, device).start()
                 self.counts[g] += 1
             if self.passed is not None:
-                level = min(da, 4 - da) + min(db, 4 - db)
-                remote(block, block, self.sent.at[g], self.passed.at[level], partner).start()
+                remote(block, block, self.sent.at[g], self.passed, partner).start()
                 self.counts[g] += 1
 
         def start(self, g):
-            self.fire(g, 0, 0, "b+", "b-", "a+", "a-")
-
-        def take(self, g, da, db):
-            arrive(self.block(g, da, db), self.arrived.at[g, 4 * da + db])
-            ways = []
-            if db == 0:
-                if da == (3 if g == 0 else 1):
-                    ways.append("a+" if g == 0 else "a-")
-                ways += ["b+", "b-"]
-            elif db == (3 if (da in (0, 1)) == (g == 0) else 1):
-                ways.append("b+" if db == 3 else "b-")
-            self.fire(g, da, db, *ways)
-
-        def take_level(self, level, parts=(0, 1)):
-            for g in parts:
-                for da, db in LEVELS[level]:
-                    self.take(g, da, db)
+            for s in range(self.parts):
+                self.fire(g, s, 0, 0, "b+", "b-", "a+", "a-")
+
+        def take(self, g, s, group):
+            whole = self.blocks.at[pl.ds(0, len(group)), pl.ds(0, self.size)]
+            arrive(whole, self.arrived.at[self.parts * g + s, GROUP_OF[group[0]]])
+            even = (g + s) % 2 == 0
+            for da, db in group:
+                ways = []
+                if db == 0:
+                    if da == (3 if even else 1):
+                        ways.append("a+" if even else "a-")
+                    ways += ["b+", "b-"]
+                elif db == (3 if (da in (0, 1)) == even else 1):
+                    ways.append("b+" if db == 3 else "b-")
+                self.fire(g, s, da, db, *ways)
+
+        def take_level(self, level, only=None):
+            for g, s in self.pieces:
+                if only in (None, g):
+                    for group in GROUPS[level]:
+                        self.take(g, s, group)
 
         def finish(self):
             for g in (0, 1):
-                sent_off(self.blocks.at[pl.ds(0, self.counts[g])], self.sent.at[g])
+                sent_off(self.blocks.at[pl.ds(0, self.counts[g] // self.parts)], self.sent.at[g])
 
     loaded(0, factors.at[mine])
-    gather = Gather(0, 0, factors)
+    gather = Gather(0, recv_sem, factors, 2)
     gather.start(0)
     pl.when(c == 0)(lambda: hand_later(output_args, weight_output, rows))
     pl.when(c == 1)(lambda: hand_later(value_args, weight_value, columns))
-    for copy in load_maps:
-        copy.wait()
+    loaded(4, maps)
+    loaded(5, lam)
+    loaded(6, gain)
     width = COLS // HEADS_HERE
     for h in range(HEADS_HERE):
         span = pl.ds(h * width, width)
@@ -200,7 +212,7 @@
         rights[1, :, span] = (scaled * gain[span][None, :]).astype(bf16)
     arrive(factors.at[mine], in_sem.at[0])
     gather.start(1)
-    loaded(8, rights.at[0])
+    loaded(7, rights.at[0])
     hand(4, rights.at[1 - c], right_in)
 
     def project(t, *chips, fresh=False):
@@ -226,30 +238,30 @@
     gather.take_level(1)
     loaded(1, wide.at[0])
     project(0, own, fresh=True)
-    gather.take_level(2, (0,))
+    gather.take_level(2, 0)
     project_pairs(0, 1, 0)
-    gather.take_level(2, (1,))
+    gather.take_level(2, 1)
     project_pairs(0, 1, 1)
-    gather.take_level(3, (0,))
+    gather.take_level(3, 0)
     arrive(wide.at[1], in_sem.at[1])
     project(1, own, fresh=True)
-    project_pairs(1, 1, 0)
+    project_pairs(1, 1, 0, 1)
+    gather.take_level(3, 1)
     loaded(2, moments.at[mine])
     arrive(moments.at[mine], in_sem.at[2])
-    moment_gather = Gather(1, 1, moments)
+    moment_gather = Gather(1, moment_sem, moments, 1)
     moment_gather.start(0)
     moment_gather.start(1)
-    gather.take_level(3, (1,))
-    project_pairs(1, 1, 1)
     project_pairs(0, 2, 0, 1, 2)
-    project_pairs(1, 2, 0)
-    project_pairs(1, 2, 1, 2)
-    project_pairs(0, 3, 0, 1)
+    project_pairs(1, 2, 0, 1)
     gather.take_level(4)
+    project_pairs(1, 2, 2)
+    for t in (0, 1):
+        project_pairs(t, 3, 0, 1)
     moment_gather.take_level(1)
-    project_pairs(1, 3, 0, 1)
     for t in (0, 1):
         project(t, at(2, 2))
+
     arrive(right_in, in_sem.at[4])
     product = None
     for t in (0, 1):
@@ -340,7 +352,7 @@
         + jnp.dot(left, ratios[1], preferred_element_type=f32)
     ).reshape(2, LANES, COLS)
 
-    spread = Gather(2, 0, copies.at[c], pass_sem)
+    spread = Gather(2, recv_sem, copies.at[c], 2, passed=pass_sem.at[0])
     for g in (0, 1):
         core = c if g == 0 else 1 - c
         for j in range(4):
@@ -382,33 +394,25 @@
     sent_off(back_moved, out_sem.at[6])
     arrive(back, in_sem.at[5])
     arrive(back_moved, in_sem.at[6])
-    for level in range(5):
-        arrive(copies.at[0, pl.ds(0, 2 * len(LEVELS[level]))], pass_sem.at[level])
+    arrive(copies.at[0], pass_sem.at[0])
     spread.finish()
 
 
 def write_kernel(new_weights, moved, copies, *rest):
     outs, sem = rest[:8], rest[8]
     new_v, first_v, second_v, copy_v, new_o, first_o, second_o, copy_o = outs
-    pairs = []
     for j in range(4):
         span = pl.ds(LANES * j, LANES)
-        pairs.append((copies.at[0, :, span], copy_v.at[:, :, span]))
-        pairs.append((new_weights.at[0, span], new_v.at[:, span]))
+        pltpu.make_async_copy(copies.at[0, :, span], copy_v.at[:, :, span], sem.at[0]).start()
+        pltpu.make_async_copy(new_weights.at[0, span], new_v.at[:, span], sem.at[1]).start()
     for k in range(2 * CHIPS):
-        pairs.append((copies.at[1, k], copy_o.at[:, pl.ds(LANES * k, LANES)]))
-    pairs += [
-        (new_weights.at[1], new_o),
-        (moved.at[0, 0], first_v),
-        (moved.at[0, 1], second_v),
-        (moved.at[1, 0], first_o),
-        (moved.at[1, 1], second_o),
-    ]
-    started = [pltpu.make_async_copy(s, t, sem.at[k]) for k, (s, t) in enumerate(pairs)]
-    for copy in started:
-        copy.start()
-    for copy in started:
-        copy.wait()
+        target = copy_o.at[:, pl.ds(LANES * k, LANES)]
+        pltpu.make_async_copy(copies.at[1, k], target, sem.at[0]).start()
+    pltpu.make_async_copy(new_weights.at[1], new_o, sem.at[1]).start()
+    for k, target in enumerate((first_v, second_v, first_o, second_o)):
+        pltpu.make_async_copy(moved.at[k // 2, k % 2], target, sem.at[2]).start()
+    for k, source in enumerate((copies, new_weights, moved)):
+        pltpu.make_async_copy(source, source, sem.at[k]).wait()
 
 
 def shards(*args):
@@ -446,12 +450,13 @@
             pltpu.VMEM((2, LANES, COLS), f32),
             pltpu.VMEM((COLS, LANES), f32),
             pltpu.VMEM((2, 8, COLS), f32),
-            dma((9,)),
+            dma((8,)),
             dma((7,)),
             dma((7,)),
             dma((3, 2)),
-            dma((2, 2, 16)),
-            dma((5,)),
+            dma((4, 8)),
+            dma((2, 8)),
+            dma((1,)),
             dma((2,)),
             dma((2, 2)),
             dma((2, 2)),
@@ -475,7 +480,7 @@
         ),
         in_specs=[vmem] * 3,
         out_specs=(hbm,) * 8,
-        scratch_shapes=[dma((2 * CHIPS + 13,))],
+        scratch_shapes=[dma((3,))],
         compiler_params=pltpu.CompilerParams(vmem_limit_bytes=4 * 1024 * 1024),
         name="write",
     )(*passed)

time: 77.5 us -> 75.2 us (0.970)
  Pallas kernels: 76.8 us -> 74.4 us
    pallas_call x1, Pallas kernels: 72.9 us -> 71 us  [shards(): pl.pallas_call(step_kernel, out_shape=(pltpu.VMEM((2, COLS, LANES), f32),...]
where the time goes in v4:
time: 75.2 us; the launch traced here: 75 us
  Pallas kernels  74.4 us (99%)
    pallas_call x1, Pallas kernels, shards(): pl.pallas_call(step_kernel, out_shape=(pltpu.VMEM((2, COLS, LANES), f32),...  71 us
    pallas_call x1, Pallas kernels, shards(): pl.pallas_call(write_kernel, out_shape=(jax.ShapeDtypeStruct((LANES, COLS...  3.45 us

profile of v4, /device:TPU:1, one launch (start us, length us, event | category | flops | bytes accessed | tf_op | source)
XLA Modules:
  0.0 75.0 jit_solution(8707677610934719439)
XLA Ops:
  0.6 71.0 %step.1 = (f32[2,512,128]{2,1,0:T(8,128)S(1)}, f32[2,2,8,512]{3,2,1,0:T(8,128)S(1)}, bf16[2,32,512,128]{3,2,1,0:T(8,128)(2,1)S(1)}) custom-call(bf16[768,512]{1,0:T(8,128)(2,1)} %first_map.1, bf16[768,512]{1,0:T(8,128)(2,1)} %second_map.1, f32[4]{0:T(128)} %lambda_head.1, f32[512]{0:T(512)} %head_gain.1, bf16[768,4096]{1,0:T(8,128)(2,1)} %cot_output.1, ...), custom_call_target="tpu_custom_call" | custom-call | tf_op jit(solution)/shard_map/step/pallas_call | solution.py:422
  71.6 3.4 %write.1 = (f32[128,512]{1,0:T(8,128)}, f32[8,512]{1,0:T(8,128)}, f32[8,512]{1,0:T(8,128)}, bf16[32,128,512]{2,1,0:T(8,128)(2,1)}, f32[512,128]{1,0:T(8,128)}, /...) custom-call(f32[2,512,128]{2,1,0:T(8,128)S(1)} %get-tuple-element.19.new_weights, ...), custom_call_target="tpu_custom_call" | custom-call | tf_op jit(solution)/shard_map/write/pallas_call | solution.py:469

commit v5 on v4

--- a/solution.py
+++ b/solution.py
@@ -50,7 +50,7 @@
     factor_value, factor_output, weight_value, weight_output,
     first_value, second_value, first_output, second_output,
     new_weights, moved, copies,
-    maps, lam, gain, wide, rights, right_in, factors, weights, moments,
+    maps, lam, gain, wide, rights, right_in, factors, other_rows, weights, moments,
     acc, turned, summed, cross_in, squares, cross_sq, last_sq, low_all, ratios, added, back, back_moved,
     load_sem, out_sem, in_sem, send_sem, recv_sem, moment_sem, pass_sem, cross_sem, sq_sem, low_sem,
 ):
@@ -91,8 +91,8 @@
     def loaded(k, target):
         pltpu.make_async_copy(target, target, load_sem.at[k]).wait()
 
-    value_args = (factor_value, first_value, second_value, layer_input)
-    output_args = (factor_output, first_output, second_output, cot_output)
+    value_args = (first_value, second_value, layer_input)
+    output_args = (first_output, second_output, cot_output)
 
     def columns(ref, j):
         return ref.at[:, pl.ds(LANES * j, LANES)]
@@ -100,18 +100,19 @@
     def rows(ref, j):
         return ref.at[pl.ds(LANES * j, LANES)]
 
-    def load_first(args):
-        load(0, args[0], factors.at[mine])
+    def load_first(own_factor, other_factor):
+        load(0, own_factor, factors.at[mine])
+        load(8, other_factor, other_rows)
 
     def load_later(args, weight, pieces):
-        load(1, args[3], wide.at[0])
-        load(2, args[1], moments.at[mine, 0])
-        load(2, args[2], moments.at[mine, 1])
+        load(1, args[2], wide.at[0])
+        load(2, args[0], moments.at[mine, 0])
+        load(2, args[1], moments.at[mine, 1])
         for j in range(4):
             load(3, pieces(weight, j), rows(weights.at[c], j))
 
-    pl.when(c == 0)(lambda: load_first(value_args))
-    pl.when(c == 1)(lambda: load_first(output_args))
+    pl.when(c == 0)(lambda: load_first(factor_value, factor_output))
+    pl.when(c == 1)(lambda: load_first(factor_output, factor_value))
     barrier = pltpu.get_barrier_semaphore()
     greeted = [chip_at(1, 0), chip_at(3, 0), chip_at(0, 1), chip_at(0, 3), partner]
     greeted += [near(0, 0, dc, dx) for dx in (1, 2, 3) for dc in (0, 1)]
@@ -130,14 +131,14 @@
         remote(source, target, out_sem.at[k], in_sem.at[k], partner).start()
 
     def hand_later(args, weight, pieces):
-        hand(1, args[3], wide.at[1])
-        hand(2, args[1], moments.at[mine, 0])
-        hand(2, args[2], moments.at[mine, 1])
+        hand(1, args[2], wide.at[1])
+        hand(2, args[0], moments.at[mine, 0])
+        hand(2, args[1], moments.at[mine, 1])
         for j in range(4):
             hand(3, pieces(weight, j), rows(weights.at[c], j))
 
-    pl.when(c == 0)(lambda: hand(0, factor_output, factors.at[mine]))
-    pl.when(c == 1)(lambda: hand(0, factor_value, factors.at[mine]))
+    loaded(8, other_rows)
+    hand(0, other_rows, factors.at[mine])
 
     class Gather:
         def __init__(self, stage, arrived, blocks, parts, passed=None):
@@ -253,12 +254,10 @@
     moment_gather.start(0)
     moment_gather.start(1)
     project_pairs(0, 2, 0, 1, 2)
-    project_pairs(1, 2, 0, 1)
-    gather.take_level(4)
-    project_pairs(1, 2, 2)
+    project_pairs(1, 2, 0, 1, 2)
     for t in (0, 1):
         project_pairs(t, 3, 0, 1)
-    moment_gather.take_level(1)
+    gather.take_level(4)
     for t in (0, 1):
         project(t, at(2, 2))
 
@@ -283,6 +282,7 @@
             summed.at[at(dz, dy)], cross_in.at[k], cross_sem.at[0], cross_sem.at[1],
             near(dz, dy, 0, 0),
         ).start()
+    moment_gather.take_level(1)
     arrive(cross_in, cross_sem.at[1])
     total = summed[own]
     for k in range(len(offsets)):
@@ -306,9 +306,6 @@
     send_low(low_all.at[own], 0)
     send_low(low_all.at[own], 1)
     moment_gather.take_level(2)
-    arrive(low_all.at[pl.ds(0, 3)], low_sem.at[0, 1])
-    for k in (2, 1, 3):
-        send_low(low_all.at[place(k, 0)], 1)
     arrive(cross_sq, sq_sem.at[0, 1])
     plane = squares[0]
     for k in range(len(offsets)):
@@ -318,6 +315,9 @@
         remote(
             squares.at[1], last_sq.at[k], sq_sem.at[1, 0], sq_sem.at[1, 1], near(0, 0, dc, dx)
         ).start()
+    arrive(low_all.at[pl.ds(0, 3)], low_sem.at[0, 1])
+    for k in (2, 1, 3):
+        send_low(low_all.at[place(k, 0)], 1)
     moment_gather.take_level(3)
     arrive(weights.at[0], in_sem.at[3])
     loaded(3, weights.at[0])
@@ -436,6 +436,7 @@
             pltpu.VMEM((2, ROWS, COLS), bf16),
             pltpu.VMEM((ROWS, COLS), bf16),
             pltpu.VMEM((2 * CHIPS, LANES, RANK), bf16),
+            pltpu.VMEM((LANES, RANK), bf16),
             pltpu.VMEM((2, COLS, LANES), f32),
             pltpu.VMEM((2 * CHIPS, 2, 8, COLS), f32),
             pltpu.VMEM((2, ROWS, RANK), f32),
@@ -450,7 +451,7 @@
             pltpu.VMEM((2, LANES, COLS), f32),
             pltpu.VMEM((COLS, LANES), f32),
             pltpu.VMEM((2, 8, COLS), f32),
-            dma((8,)),
+            dma((9,)),
             dma((7,)),
             dma((7,)),
             dma((3, 2)),

time: 75.2 us -> 74.1 us (0.985)
  Pallas kernels: 74.4 us -> 73.3 us
    pallas_call x1, Pallas kernels: 71 us -> 69.9 us  [shards(): pl.pallas_call(step_kernel, out_shape=(pltpu.VMEM((2, COLS, LANES), f32),...]
where the time goes in v5:
time: 74.1 us; the launch traced here: 74 us
  Pallas kernels  73.3 us (99%)
    pallas_call x1, Pallas kernels, shards(): pl.pallas_call(step_kernel, out_shape=(pltpu.VMEM((2, COLS, LANES), f32),...  69.9 us
    pallas_call x1, Pallas kernels, shards(): pl.pallas_call(write_kernel, out_shape=(jax.ShapeDtypeStruct((LANES, COLS...  3.45 us

profile of v5, /device:TPU:1, one launch (start us, length us, event | category | flops | bytes accessed | tf_op | source)
XLA Modules:
  0.0 74.0 jit_solution(14265399211250848263)
XLA Ops:
  0.6 69.9 %step.1 = (f32[2,512,128]{2,1,0:T(8,128)S(1)}, f32[2,2,8,512]{3,2,1,0:T(8,128)S(1)}, bf16[2,32,512,128]{3,2,1,0:T(8,128)(2,1)S(1)}) custom-call(bf16[768,512]{1,0:T(8,128)(2,1)} %first_map.1, bf16[768,512]{1,0:T(8,128)(2,1)} %second_map.1, f32[4]{0:T(128)} %lambda_head.1, f32[512]{0:T(512)} %head_gain.1, bf16[768,4096]{1,0:T(8,128)(2,1)} %cot_output.1, ...), custom_call_target="tpu_custom_call" | custom-call | tf_op jit(solution)/shard_map/step/pallas_call | solution.py:422
  70.5 3.4 %write.1 = (f32[128,512]{1,0:T(8,128)}, f32[8,512]{1,0:T(8,128)}, f32[8,512]{1,0:T(8,128)}, bf16[32,128,512]{2,1,0:T(8,128)(2,1)}, f32[512,128]{1,0:T(8,128)}, /...) custom-call(f32[2,512,128]{2,1,0:T(8,128)S(1)} %get-tuple-element.19.new_weights, ...), custom_call_target="tpu_custom_call" | custom-call | tf_op jit(solution)/shard_map/write/pallas_call | solution.py:470

commit v6 on v5

--- a/solution.py
+++ b/solution.py
@@ -115,7 +115,7 @@
     pl.when(c == 1)(lambda: load_first(factor_output, factor_value))
     barrier = pltpu.get_barrier_semaphore()
     greeted = [chip_at(1, 0), chip_at(3, 0), chip_at(0, 1), chip_at(0, 3), partner]
-    greeted += [near(0, 0, dc, dx) for dx in (1, 2, 3) for dc in (0, 1)]
+    greeted += [near(0, 0, 0, dx) for dx in (1, 2, 3)]
     for device in greeted:
         pl.semaphore_signal(barrier, inc=1, device_id=device, device_id_type=MESH)
     load(4, first_map, maps.at[0])
@@ -168,9 +168,8 @@
                 remote(block, block, self.sent.at[g], self.passed, partner).start()
                 self.counts[g] += 1
 
-        def start(self, g):
-            for s in range(self.parts):
-                self.fire(g, s, 0, 0, "b+", "b-", "a+", "a-")
+        def start(self, g, s):
+            self.fire(g, s, 0, 0, "b+", "b-", "a+", "a-")
 
         def take(self, g, s, group):
             whole = self.blocks.at[pl.ds(0, len(group)), pl.ds(0, self.size)]
@@ -198,7 +197,8 @@
 
     loaded(0, factors.at[mine])
     gather = Gather(0, recv_sem, factors, 2)
-    gather.start(0)
+    gather.start(0, 0)
+    gather.start(0, 1)
     pl.when(c == 0)(lambda: hand_later(output_args, weight_output, rows))
     pl.when(c == 1)(lambda: hand_later(value_args, weight_value, columns))
     loaded(4, maps)
@@ -212,7 +212,8 @@
         scaled = differ * lax.rsqrt(mean + norm_epsilon)
         rights[1, :, span] = (scaled * gain[span][None, :]).astype(bf16)
     arrive(factors.at[mine], in_sem.at[0])
-    gather.start(1)
+    gather.start(1, 0)
+    gather.start(1, 1)
     loaded(7, rights.at[0])
     hand(4, rights.at[1 - c], right_in)
 
@@ -251,8 +252,8 @@
     loaded(2, moments.at[mine])
     arrive(moments.at[mine], in_sem.at[2])
     moment_gather = Gather(1, moment_sem, moments, 1)
-    moment_gather.start(0)
-    moment_gather.start(1)
+    moment_gather.start(0, 0)
+    moment_gather.start(1, 0)
     project_pairs(0, 2, 0, 1, 2)
     project_pairs(1, 2, 0, 1, 2)
     for t in (0, 1):
@@ -293,10 +294,11 @@
         value = value[:8] + value[8:]
         return sum(value[:, LANES * j : LANES * (j + 1)] for j in range(COLS // LANES))
 
-    squares[0] = fold(total * total)
-    for k, (dz, dy) in enumerate(offsets):
+    squares[0, :1] = jnp.sum(fold(total * total), axis=0, keepdims=True)
+    everyone = [(dz, dy, dc) for dz, dy in offsets for dc in (1, 0)] + [(0, 0, 1)]
+    for k, (dz, dy, dc) in enumerate(everyone):
         remote(
-            squares.at[0], cross_sq.at[k], sq_sem.at[0, 0], sq_sem.at[0, 1], near(dz, dy, 0, 0)
+            squares.at[0, pl.ds(0, 1)], cross_sq.at[pl.ds(k, 1)], sq_sem.at[0, 0], sq_sem.at[0, 1], near(dz, dy, dc, 0)
         ).start()
     def send_low(block, way):
         for by in (2, 1, 3):
@@ -306,27 +308,23 @@
     send_low(low_all.at[own], 0)
     send_low(low_all.at[own], 1)
     moment_gather.take_level(2)
-    arrive(cross_sq, sq_sem.at[0, 1])
-    plane = squares[0]
-    for k in range(len(offsets)):
-        plane = plane + cross_sq[k]
-    squares[1] = plane
-    for k, (dx, dc) in enumerate(((2, 1), (1, 1), (3, 1), (2, 0), (1, 0), (3, 0), (0, 1))):
-        remote(
-            squares.at[1], last_sq.at[k], sq_sem.at[1, 0], sq_sem.at[1, 1], near(0, 0, dc, dx)
-        ).start()
     arrive(low_all.at[pl.ds(0, 3)], low_sem.at[0, 1])
     for k in (2, 1, 3):
         send_low(low_all.at[place(k, 0)], 1)
+    arrive(cross_sq.at[pl.ds(0, 31)], sq_sem.at[0, 1])
+    cross_sq[31:] = squares[0, :1]
+    squares[1, :1] = jnp.sum(cross_sq[...], axis=0, keepdims=True)
+    for k, dx in enumerate((2, 1, 3)):
+        remote(
+            squares.at[1, pl.ds(0, 1)], last_sq.at[pl.ds(k, 1)], sq_sem.at[1, 0], sq_sem.at[1, 1], near(0, 0, 0, dx)
+        ).start()
     moment_gather.take_level(3)
     arrive(weights.at[0], in_sem.at[3])
     loaded(3, weights.at[0])
     arrive(low_all.at[pl.ds(0, 12)], low_sem.at[1, 1])
-    arrive(last_sq, sq_sem.at[1, 1])
-    whole = squares[1]
-    for k in range(7):
-        whole = whole + last_sq[k]
-    square_sum = jnp.sum(jnp.sum(whole, axis=1, keepdims=True), axis=0, keepdims=True)
+    arrive(last_sq.at[pl.ds(0, 3)], sq_sem.at[1, 1])
+    whole = squares[1, :1] + last_sq[0:1] + last_sq[1:2] + last_sq[2:3]
+    square_sum = jnp.sum(whole, axis=1, keepdims=True)
     clip = jnp.minimum(1.0, math.sqrt(RANK * HV) * lax.rsqrt(square_sum + norm_epsilon))
 
     moment_gather.take_level(4)
@@ -365,7 +363,8 @@
                 new_weights[c, span] = fresh
             else:
                 back[span] = fresh
-        spread.start(g)
+            if j % 2 == 1:
+                spread.start(g, j // 2)
     for g in (0, 1):
         core = c if g == 0 else 1 - c
         first_new, second_new = moved_by(
@@ -384,8 +383,8 @@
     sent_off(weights.at[0], out_sem.at[3])
     sent_off(right_in, out_sem.at[4])
     sent_off(cross_in, cross_sem.at[0])
-    sent_off(cross_sq, sq_sem.at[0, 0])
-    sent_off(last_sq, sq_sem.at[1, 0])
+    sent_off(cross_sq.at[pl.ds(0, 31)], sq_sem.at[0, 0])
+    sent_off(last_sq.at[pl.ds(0, 3)], sq_sem.at[1, 0])
     sent_off(low_all.at[pl.ds(0, 3)], low_sem.at[0, 0])
     sent_off(low_all.at[pl.ds(0, 12)], low_sem.at[1, 0])
     for level in (1, 2, 3, 4):
@@ -444,8 +443,8 @@
             pltpu.VMEM((CHIPS, 16, COLS), f32),
             pltpu.VMEM((CHIPS - 1, 16, COLS), f32),
             pltpu.VMEM((2, 8, LANES), f32),
-            pltpu.VMEM((CHIPS - 1, 8, LANES), f32),
-            pltpu.VMEM((7, 8, LANES), f32),
+            pltpu.VMEM((2 * CHIPS, LANES), f32),
+            pltpu.VMEM((8, LANES), f32),
             pltpu.VMEM((CHIPS, 16, COLS), f32),
             pltpu.VMEM((2, RANK, COLS), bf16),
             pltpu.VMEM((2, LANES, COLS), f32),

time: 74.1 us -> 73.9 us (level)
  no operation moved by 1% of the time
where the time goes in v6:
time: 73.9 us; the launch traced here: 73.8 us
  Pallas kernels  73.2 us (99%)
    pallas_call x1, Pallas kernels, shards(): pl.pallas_call(step_kernel, out_shape=(pltpu.VMEM((2, COLS, LANES), f32),...  69.7 us
    pallas_call x1, Pallas kernels, shards(): pl.pallas_call(write_kernel, out_shape=(jax.ShapeDtypeStruct((LANES, COLS...  3.45 us

profile of v6, /device:TPU:1, one launch (start us, length us, event | category | flops | bytes accessed | tf_op | source)
XLA Modules:
  0.0 73.8 jit_solution(17449293719002641112)
XLA Ops:
  0.6 69.7 %step.1 = (f32[2,512,128]{2,1,0:T(8,128)S(1)}, f32[2,2,8,512]{3,2,1,0:T(8,128)S(1)}, bf16[2,32,512,128]{3,2,1,0:T(8,128)(2,1)S(1)}) custom-call(bf16[768,512]{1,0:T(8,128)(2,1)} %first_map.1, bf16[768,512]{1,0:T(8,128)(2,1)} %second_map.1, f32[4]{0:T(128)} %lambda_head.1, f32[512]{0:T(512)} %head_gain.1, bf16[768,4096]{1,0:T(8,128)(2,1)} %cot_output.1, ...), custom_call_target="tpu_custom_call" | custom-call | tf_op jit(solution)/shard_map/step/pallas_call | solution.py:421
  70.4 3.4 %write.1 = (f32[128,512]{1,0:T(8,128)}, f32[8,512]{1,0:T(8,128)}, f32[8,512]{1,0:T(8,128)}, bf16[32,128,512]{2,1,0:T(8,128)(2,1)}, f32[512,128]{1,0:T(8,128)}, /...) custom-call(f32[2,512,128]{2,1,0:T(8,128)S(1)} %get-tuple-element.19.new_weights, ...), custom_call_target="tpu_custom_call" | custom-call | tf_op jit(solution)/shard_map/write/pallas_call | solution.py:469

commit v7 on v5

--- a/solution.py
+++ b/solution.py
@@ -257,13 +257,11 @@
     project_pairs(1, 2, 0, 1, 2)
     for t in (0, 1):
         project_pairs(t, 3, 0, 1)
+    arrive(right_in, in_sem.at[4])
     gather.take_level(4)
+    product = None
     for t in (0, 1):
         project(t, at(2, 2))
-
-    arrive(right_in, in_sem.at[4])
-    product = None
-    for t in (0, 1):
         flat = acc[t].T
         high = flat.astype(bf16)
         turned[t, :RANK] = high

time: 74.1 us -> 73.9 us (level)
  no operation moved by 1% of the time
where the time goes in v7:
time: 73.9 us; the launch traced here: 73.8 us
  Pallas kernels  73.1 us (99%)
    pallas_call x1, Pallas kernels, shards(): pl.pallas_call(step_kernel, out_shape=(pltpu.VMEM((2, COLS, LANES), f32),...  69.7 us
    pallas_call x1, Pallas kernels, shards(): pl.pallas_call(write_kernel, out_shape=(jax.ShapeDtypeStruct((LANES, COLS...  3.45 us

profile of v7, /device:TPU:1, one launch (start us, length us, event | category | flops | bytes accessed | tf_op | source)
XLA Modules:
  0.0 73.8 jit_solution(824730945121010101)
XLA Ops:
  0.6 69.7 %step.1 = (f32[2,512,128]{2,1,0:T(8,128)S(1)}, f32[2,2,8,512]{3,2,1,0:T(8,128)S(1)}, bf16[2,32,512,128]{3,2,1,0:T(8,128)(2,1)S(1)}) custom-call(bf16[768,512]{1,0:T(8,128)(2,1)} %first_map.1, bf16[768,512]{1,0:T(8,128)(2,1)} %second_map.1, f32[4]{0:T(128)} %lambda_head.1, f32[512]{0:T(512)} %head_gain.1, bf16[768,4096]{1,0:T(8,128)(2,1)} %cot_output.1, ...), custom_call_target="tpu_custom_call" | custom-call | tf_op jit(solution)/shard_map/step/pallas_call | solution.py:420
  70.3 3.4 %write.1 = (f32[128,512]{1,0:T(8,128)}, f32[8,512]{1,0:T(8,128)}, f32[8,512]{1,0:T(8,128)}, bf16[32,128,512]{2,1,0:T(8,128)(2,1)}, f32[512,128]{1,0:T(8,128)}, /...) custom-call(f32[2,512,128]{2,1,0:T(8,128)S(1)} %get-tuple-element.19.new_weights, ...), custom_call_target="tpu_custom_call" | custom-call | tf_op jit(solution)/shard_map/write/pallas_call | solution.py:468
